TPU v7x, 256 devices: a whole 4x4x8 slice. The times are simulated.
256 devices in a mesh: ep: 16 (over y, x), tp: 16 (over z, core).
Axes of the slice: x: 4, y: 4, z: 8, core: 2. Of those that a mesh axis runs over, the one named last changes fastest.
Arguments:
- hidden_in: bfloat16 [256, 4096], P('ep'), may hold values from -6 to 6
- attn_gain: float32 [4096], replicated, may hold values from 0.1 to 1.9
- query_weight: bfloat16 [4096, 4096], P('ep', 'tp'), may hold values from -0.09375 to 0.09375
- key_weight: bfloat16 [4096, 2048], P('ep', 'tp'), may hold values from -0.09375 to 0.09375
- value_weight: bfloat16 [4096, 2048], P('ep', 'tp'), may hold values from -0.09375 to 0.09375
- query_gain: float32 [128], replicated, may hold values from 0.1 to 1.9
- key_gain: float32 [128], replicated, may hold values from 0.1 to 1.9
- head_offset: float32 [32], P('tp'), may hold values from -7 to -2
- key_cache: bfloat16 [256, 1024, 2048], P('ep', None, 'tp'), may hold values from -6 to 6
- value_cache: bfloat16 [256, 1024, 2048], P('ep', None, 'tp'), may hold values from -6 to 6
- lengths: int32 [256], P('ep'), may hold values from 1 to 1024
- out_weight: bfloat16 [4096, 4096], P('tp', 'ep'), may hold values from -0.375 to 0.375
- expert_gain: float32 [4096], replicated, may hold values from 0.1 to 1.9
- routes: int32 [256, 2], P('ep'), may hold values from 0 to 15, all different within a row; in each aligned block of 16 rows (0 to 15, 16 to 31, ...) at most 4 rows name the same one
- route_weights: float32 [256, 2], P('ep'), may hold values from 0.1 to 1
- gate_weight: bfloat16 [16, 4096, 2048], P('ep', None, 'tp'), may hold values from -0.09375 to 0.09375
- up_weight: bfloat16 [16, 4096, 2048], P('ep', None, 'tp'), may hold values from -0.09375 to 0.09375
- down_weight: bfloat16 [16, 2048, 4096], P('ep', 'tp'), may hold values from -0.125 to 0.125
Outputs:
- layer_out: bfloat16 [256, 4096], P('ep', 'tp')
- fresh_keys: bfloat16 [256, 2048], P('ep', 'tp')
- fresh_values: bfloat16 [256, 2048], P('ep', 'tp')
Inputs may be any that keep to these rules, and one draw needn't show every extreme that they name: `routes`: each row names 2 different experts. Among the rows of one index of ep (16 rows) no expert is named more than 4 times, a bound that some block reaches.
All inputs are finite; a program needn't handle non-finite values.
Results may differ from a plain program's by a relative error of at most 0.018.
Values may be sent and summed in bfloat16 or wider, within the bound.
A program may use at most 64 MiB of HBM per device.

v0:
```python
import jax
import jax.numpy as jnp
from jax import lax
from jax.sharding import PartitionSpec as P

EPSILON = 1e-06


def split_up(shard, dim, size):
    shape = shard.shape
    tiles = shard.reshape(*shape[:dim], size, shape[dim] // size, *shape[dim + 1 :])
    return jnp.moveaxis(tiles, dim, 0)


def sent_and_summed(shard, axis, dim):
    size = lax.axis_size(axis)
    tiles = lax.all_to_all(split_up(shard, dim, size), axis, 0, 0, tiled=True)
    return jnp.sum(tiles.astype(jnp.float32), axis=0)


def joined_along(tiles, dim):
    tiles = jnp.moveaxis(tiles, 0, dim)
    shape = tiles.shape
    return tiles.reshape(*shape[:dim], shape[dim] * shape[dim + 1], *shape[dim + 2 :])


def sent_to_all(shard, axis):
    size = lax.axis_size(axis)
    return lax.all_to_all(
        jnp.broadcast_to(shard[None], (size, *shard.shape)), axis, 0, 0, tiled=True
    )


def gather_directly(shard, axis, dim):
    return joined_along(sent_to_all(shard, axis), dim)


def over_copies(shard, axis):
    return sent_to_all(shard, axis).sum(axis=0)


def norm_rows(values, gain):
    meansq = jnp.mean(values * values, axis=-1, keepdims=True)
    return values * lax.rsqrt(meansq + EPSILON) * gain


def body(
    hidden_in,
    attn_gain,
    query_weight,
    key_weight,
    value_weight,
    query_gain,
    key_gain,
    head_offset,
    key_cache,
    value_cache,
    lengths,
    out_weight,
    expert_gain,
    routes,
    route_weights,
    gate_weight,
    up_weight,
    down_weight,
):
    count_ep = lax.axis_size("ep")
    count_tp = lax.axis_size("tp")
    seqs_here = hidden_in.shape[0]
    width = hidden_in.shape[1]
    head_dim = query_gain.shape[0]
    query_cols = query_weight.shape[1]
    pair_cols = key_weight.shape[1]
    kv_here = pair_cols // head_dim
    groups = query_cols // pair_cols
    cache_len = key_cache.shape[1]
    x_float = hidden_in.astype(jnp.float32)
    normed = norm_rows(x_float, attn_gain).astype(jnp.bfloat16)
    slices = lax.all_to_all(normed, "ep", split_axis=1, concat_axis=0, tiled=True)
    summed = sent_and_summed(
        jnp.concatenate(
            [
                jnp.dot(slices, query_weight, preferred_element_type=jnp.float32),
                jnp.dot(slices, key_weight, preferred_element_type=jnp.float32),
                jnp.dot(slices, value_weight, preferred_element_type=jnp.float32),
            ],
            axis=1,
        ).astype(jnp.bfloat16),
        "ep",
        0,
    )
    query_raw = summed[:, :query_cols].astype(jnp.bfloat16)
    key_raw = summed[:, query_cols : query_cols + pair_cols].astype(jnp.bfloat16)
    fresh_values = summed[:, query_cols + pair_cols :].astype(jnp.bfloat16)
    query = norm_rows(
        query_raw.astype(jnp.float32).reshape(seqs_here, query_cols // head_dim, head_dim),
        query_gain,
    ).astype(jnp.bfloat16)
    fresh_keys = norm_rows(
        key_raw.astype(jnp.float32).reshape(seqs_here, kv_here, head_dim), key_gain
    ).astype(jnp.bfloat16)
    grouped = query.reshape(seqs_here, kv_here, groups, head_dim)
    cached_keys = key_cache.reshape(seqs_here, cache_len, kv_here, head_dim)
    cached_values = value_cache.reshape(seqs_here, cache_len, kv_here, head_dim)
    scores = jnp.einsum("bkgd,bskd->bkgs", grouped, cached_keys, preferred_element_type=jnp.float32)
    scores = scores * head_dim ** (-0.5) + head_offset.reshape(kv_here, groups)[None, :, :, None]
    positions = lax.broadcasted_iota(jnp.int32, (1, 1, 1, cache_len), 3)
    live = positions < lengths[:, None, None, None]
    breaks = jnp.where(live, jax.nn.softplus(scores), 0.0)
    suffix = lax.cumsum(breaks, axis=3, reverse=True) - breaks
    stick = jnp.where(live, jnp.exp(jax.nn.log_sigmoid(scores) - suffix), 0.0).astype(jnp.bfloat16)
    attended = jnp.einsum(
        "bkgs,bskd->bkgd", stick, cached_values, preferred_element_type=jnp.float32
    )
    attended = attended.astype(jnp.bfloat16).reshape(seqs_here, query_cols)
    terms = jnp.dot(
        gather_directly(attended, "ep", 0), out_weight, preferred_element_type=jnp.float32
    )
    partial_value = lax.all_to_all(
        terms.astype(jnp.bfloat16), "ep", split_axis=0, concat_axis=1, tiled=True
    ).astype(terms.dtype)
    top = routes.shape[1]
    capacity = seqs_here * top * 2 // count_ep
    slots_all = count_ep * capacity
    flat = routes.reshape(-1)
    onehot = (flat[:, None] == lax.broadcasted_iota(jnp.int32, (1, count_ep), 1)).astype(jnp.int32)
    before = jnp.cumsum(onehot, axis=0) - onehot
    rank = jnp.sum(before * onehot, axis=1)
    slot = flat * capacity + rank
    match = (slot[:, None] == lax.broadcasted_iota(jnp.int32, (1, slots_all), 1)).astype(
        jnp.float32
    )
    match = match.reshape(seqs_here, top, slots_all)
    dispatch = jnp.sum(match, axis=1).astype(jnp.bfloat16)
    combine = jnp.sum(match * route_weights[:, :, None], axis=1)
    share_width = width // count_tp
    col_start = lax.axis_index("tp") * share_width
    projected_share = sent_and_summed(partial_value.astype(jnp.bfloat16), "tp", 1)
    own_share = lax.dynamic_slice_in_dim(x_float, col_start, share_width, 1)
    residual_share = (own_share + projected_share).astype(jnp.bfloat16)
    share_float = residual_share.astype(jnp.float32)
    squares = over_copies(jnp.sum(share_float * share_float, axis=1), "tp")
    gain_share = lax.dynamic_slice_in_dim(expert_gain, col_start, share_width, 0)
    expert_share = (
        share_float * lax.rsqrt(squares / width + EPSILON)[:, None] * gain_share
    ).astype(jnp.bfloat16)
    outgoing = jnp.einsum(
        "sj,sd->jd", dispatch, expert_share, preferred_element_type=jnp.float32
    ).astype(jnp.bfloat16)
    moved = lax.all_to_all(outgoing, "ep", split_axis=0, concat_axis=0, tiled=True)
    arrived = lax.all_gather(moved, "tp", axis=1, tiled=True)
    gate = jnp.dot(arrived, gate_weight[0], preferred_element_type=jnp.float32)
    upward = jnp.dot(arrived, up_weight[0], preferred_element_type=jnp.float32)
    hidden = (jax.nn.silu(gate) * upward).astype(jnp.bfloat16)
    expert_terms = jnp.dot(hidden, down_weight[0], preferred_element_type=jnp.float32)
    expert_out = sent_and_summed(expert_terms.astype(jnp.bfloat16), "tp", 1).astype(jnp.bfloat16)
    returned = lax.all_to_all(expert_out, "ep", split_axis=0, concat_axis=0, tiled=True)
    mixed = jnp.dot(combine, returned.astype(jnp.float32), precision=lax.Precision.HIGHEST)
    layer_out = (residual_share.astype(jnp.float32) + mixed).astype(jnp.bfloat16)
    return (layer_out, fresh_keys.reshape(seqs_here, pair_cols), fresh_values)


def solution(mesh):
    placed = (
        P("ep", None),
        P(),
        P("ep", "tp"),
        P("ep", "tp"),
        P("ep", "tp"),
        P(),
        P(),
        P("tp"),
        P("ep", None, "tp"),
        P("ep", None, "tp"),
        P("ep"),
        P("tp", "ep"),
        P(),
        P("ep", None),
        P("ep", None),
        P("ep", None, "tp"),
        P("ep", None, "tp"),
        P("ep", "tp", None),
    )
    return jax.shard_map(
        body,
        mesh=mesh,
        in_specs=placed,
        out_specs=(P("ep", "tp"), P("ep", "tp"), P("ep", "tp")),
        check_vma=False,
    )
```

profile of v0, /device:TPU:1, one launch (start us, length us, event | category | flops | bytes accessed | tf_op | source)
XLA Modules:
  0.0 199.3 jit_solution(7542754235354447465)
XLA Ops:
  0.6 1.1 multiply_reduce_fusion
  1.8 1.0 multiply_convert_fusion
  2.8 14.2 %all_to_all.79 = bf16[16,16,256]{2,0,1:T(8,128)(2,1)S(1)} all-to-all(bf16[16,16,256]{2,0,1:T(8,128)(2,1)S(1)} %bitcast.66), channel_id=1, replica_groups=mesh['ep'=16,'tp'=16] {'ep'}, dimensions={1} | all-to-all | bytes 262144 | tf_op jit(solution)/shard_map/all_to_all | solution.py:79
  19.1 1.1 convolution_convert_fusion.2
  20.9 3.5 %all-to-all-start.1 = ((bf16[16,16,512]{2,1,0:T(8,128)(2,1)}), bf16[16,16,512]{2,1,0:T(8,128)(2,1)S(1)}, u32[]{:S(2)}, u32[]{:S(2)}) async-start(bf16[16,16,512]{2,1,0:T(8,128)(2,1)} %pad_maximum_fusion), calls=%async_computation.1 | async-start | bytes 524288 | tf_op jit(solution)/shard_map/all_to_all | solution.py:17
  25.2 6.8 %all-to-all-done.1 = bf16[16,16,512]{2,1,0:T(8,128)(2,1)S(1)} async-done(((bf16[16,16,512]{2,1,0:T(8,128)(2,1)}), bf16[16,16,512]{2,1,0:T(8,128)(2,1)S(1)}, u32[]{:S(2)}, u32[]{:S(2)}) %all-to-all-start.1) | async-done | bytes 262176 | tf_op jit(solution)/shard_map/all_to_all | solution.py:17
  32.2 3.4 %fusion.11 = (f32[16,2,1024]{2,1,0:T(2,128)S(1)}, f32[16,2,1024]{2,1,0:T(2,128)S(1)}) fusion(pred[16,1024]{1,0:T(8,128)(4,1)S(1)} %iota_compare_fusion, f32[2]{0:T(128)} %param.25, bf16[16,1024,128]{2,1,0:T(8,128)(2,1)} %param.26, f32[16,2,128]{2,1,0:T(2,128)S(1)} %reshape.212, f32[128]{0:T(128)} %param.23, f32[16,2]{1,0:T(8,128)S(1)} %add_rsqrt_fusion), kind=kOutput, calls=%fused_computation.27 | convolution fusion | flops 8695808 | bytes 4489864 | tf_op jit(solution)/shard_map/bkgd,bskd->bkgs/dot_general | solution.py:105
  35.8 39.6 %reduce-window.6 = f32[16,1,2,8,128]{4,3,2,1,0:T(8,128)S(1)} reduce-window(f32[16,1,2,8,128]{4,3,2,1,0:T(8,128)S(1)} %bitcast.67, f32[]{:T(128)} %constant.22.clone.1), window={size=1x1x1x1x128 pad=0_0x0_0x0_0x0_0x0_127}, to_apply=%region_3.0 | reduce-window | flops 4161536 | bytes 262148 | tf_op jit(solution)/shard_map/reduce-window
  76.0 3.4 %convolution_convert_fusion.6 = bf16[16,2,128]{2,1,0:T(2,128)(2,1)S(1)} fusion(bf16[16,1024,128]{2,1,0:T(8,128)(2,1)} %param.27, pred[16,1024]{1,0:T(8,128)(4,1)S(1)} %iota_compare_fusion, f32[16,2,1024]{2,1,0:T(2,128)S(1)} %reshape.205, f32[16,2,1024]{2,1,0:T(2,128)S(1)} %reshape.208, f32[16,2,1024]{2,1,0:T(2,128)S(1)} %get-tuple-element.8), kind=kOutput, calls=%fused_computation.12 | convolution fusion | flops 9048064 | bytes 4612096 | tf_op jit(solution)/shard_map/bkgs,bskd->bkgd/dot_general | solution.py:112
  80.0 3.5 %all-to-all-start.2 = ((bf16[16,16,256]{2,1,0:T(8,128)(2,1)}), bf16[16,16,256]{2,1,0:T(8,128)(2,1)S(1)}, u32[]{:S(2)}, u32[]{:S(2)}) async-start(bf16[16,16,256]{2,1,0:T(8,128)(2,1)} %broadcast_in_dim.22), calls=%async_computation.2 | async-start | bytes 262144 | tf_op jit(solution)/shard_map/all_to_all | solution.py:29
  83.7 6.6 %all-to-all-done.2 = bf16[16,16,256]{2,1,0:T(8,128)(2,1)S(1)} async-done(((bf16[16,16,256]{2,1,0:T(8,128)(2,1)}), bf16[16,16,256]{2,1,0:T(8,128)(2,1)S(1)}, u32[]{:S(2)}, u32[]{:S(2)}) %all-to-all-start.2) | async-done | bytes 131104 | tf_op jit(solution)/shard_map/all_to_all | solution.py:29
  91.2 4.2 %all-to-all-start.3 = ((bf16[16,16,256]{2,1,0:T(8,128)(2,1)}), bf16[16,16,256]{2,1,0:T(8,128)(2,1)}, u32[]{:S(2)}, u32[]{:S(2)}) async-start(bf16[16,16,256]{2,1,0:T(8,128)(2,1)} %bitcast.8), calls=%async_computation.3 | async-start | bytes 262144 | tf_op jit(solution)/shard_map/all_to_all | solution.py:119
  95.5 6.7 %all-to-all-done.3 = bf16[16,16,256]{2,1,0:T(8,128)(2,1)} async-done(((bf16[16,16,256]{2,1,0:T(8,128)(2,1)}), bf16[16,16,256]{2,1,0:T(8,128)(2,1)}, u32[]{:S(2)}, u32[]{:S(2)}) %all-to-all-start.3) | async-done | bytes 131104 | tf_op jit(solution)/shard_map/all_to_all | solution.py:119
  102.2 14.0 %all-to-all-start.4 = ((bf16[16,16,256]{2,1,0:T(8,128)(2,1)}), bf16[16,16,256]{2,1,0:T(8,128)(2,1)S(1)}, u32[]{:S(2)}, u32[]{:S(2)}) async-start(bf16[16,16,256]{2,1,0:T(8,128)(2,1)} %all-to-all-done.3), calls=%async_computation.4 | async-start | bytes 262144 | tf_op jit(solution)/shard_map/all_to_all | solution.py:17
  116.6 8.5 %all-to-all-done.4 = bf16[16,16,256]{2,1,0:T(8,128)(2,1)S(1)} async-done(((bf16[16,16,256]{2,1,0:T(8,128)(2,1)}), bf16[16,16,256]{2,1,0:T(8,128)(2,1)S(1)}, u32[]{:S(2)}, u32[]{:S(2)}) %all-to-all-start.4) | async-done | bytes 131104 | tf_op jit(solution)/shard_map/all_to_all | solution.py:17
  125.8 3.4 %all-to-all-start.5 = ((f32[16,1,16]{2,1,0:T(1,128)}), f32[16,1,16]{2,1,0:T(1,128)S(1)}, u32[]{:S(2)}, u32[]{:S(2)}) async-start(f32[16,1,16]{2,1,0:T(1,128)} %broadcast_in_dim.23), calls=%async_computation.5 | async-start | bytes 16384 | tf_op jit(solution)/shard_map/all_to_all | solution.py:29
  130.1 5.9 %all-to-all-done.5 = f32[16,1,16]{2,1,0:T(1,128)S(1)} async-done(((f32[16,1,16]{2,1,0:T(1,128)}), f32[16,1,16]{2,1,0:T(1,128)S(1)}, u32[]{:S(2)}, u32[]{:S(2)}) %all-to-all-start.5) | async-done | bytes 1056 | tf_op jit(solution)/shard_map/all_to_all | solution.py:29
  136.2 9.3 %all_to_all.80 = bf16[16,4,256]{2,1,0:T(4,128)(2,1)S(1)} all-to-all(bf16[16,4,256]{2,1,0:T(4,128)(2,1)S(1)} %all_to_all.63), channel_id=1, replica_groups=mesh['ep'=16,'tp'=16] {'ep'}, dimensions={0} | all-to-all | bytes 65536 | tf_op jit(solution)/shard_map/all_to_all | solution.py:150
  145.5 18.0 %all_gather.3 = bf16[64,4096]{1,0:T(8,128)(2,1)S(1)} all-gather(bf16[64,256]{1,0:T(8,128)(2,1)S(1)} %all_to_all.65), channel_id=1, replica_groups=mesh['ep'=16,'tp'=16] {'tp'}, dimensions={1}, use_global_device_ids=true | all-gather | bytes 557056 | tf_op jit(solution)/shard_map/all_gather | solution.py:151
  163.5 1.5 fusion.6
  166.6 4.2 %all-to-all-start.7 = ((bf16[16,64,256]{2,1,0:T(8,128)(2,1)}), bf16[16,64,256]{2,1,0:T(8,128)(2,1)S(1)}, u32[]{:S(2)}, u32[]{:S(2)}) async-start(bf16[16,64,256]{2,1,0:T(8,128)(2,1)} %bitcast.58), calls=%async_computation.7 | async-start | bytes 1048576 | tf_op jit(solution)/shard_map/all_to_all | solution.py:17
  170.9 17.1 %all-to-all-done.7 = bf16[16,64,256]{2,1,0:T(8,128)(2,1)S(1)} async-done(((bf16[16,64,256]{2,1,0:T(8,128)(2,1)}), bf16[16,64,256]{2,1,0:T(8,128)(2,1)S(1)}, u32[]{:S(2)}, u32[]{:S(2)}) %all-to-all-start.7) | async-done | bytes 524320 | tf_op jit(solution)/shard_map/all_to_all | solution.py:17
  188.6 3.5 %all-to-all-start.8 = ((bf16[16,4,256]{2,1,0:T(4,128)(2,1)}), bf16[16,4,256]{2,1,0:T(4,128)(2,1)S(1)}, u32[]{:S(2)}, u32[]{:S(2)}) async-start(bf16[16,4,256]{2,1,0:T(4,128)(2,1)} %all_to_all.67), calls=%async_computation.8 | async-start | bytes 65536 | tf_op jit(solution)/shard_map/all_to_all | solution.py:157
  193.4 5.1 %all-to-all-done.8 = bf16[16,4,256]{2,1,0:T(4,128)(2,1)S(1)} async-done(((bf16[16,4,256]{2,1,0:T(4,128)(2,1)}), bf16[16,4,256]{2,1,0:T(4,128)(2,1)S(1)}, u32[]{:S(2)}, u32[]{:S(2)}) %all-to-all-start.8) | async-done | bytes 32800 | tf_op jit(solution)/shard_map/all_to_all | solution.py:157
  (65 shorter events, 12.6 us)
Async XLA Ops:
  0.6 164.5 %copy-start = (bf16[1,128,4096]{2,1,0:T(8,128)(2,1)S(1)}, bf16[1,128,4096]{2,1,0:T(8,128)(2,1)}, u32[]{:S(2)}) copy-start(bf16[1,128,4096]{2,1,0:T(8,128)(2,1)} %param.35) | copy-start | bytes 3145732
  20.9 11.0 %all-to-all-start.1 = ((bf16[16,16,512]{2,1,0:T(8,128)(2,1)}), bf16[16,16,512]{2,1,0:T(8,128)(2,1)S(1)}, u32[]{:S(2)}, u32[]{:S(2)}) async-start(bf16[16,16,512]{2,1,0:T(8,128)(2,1)} %pad_maximum_fusion), calls=%async_computation.1 | async-start | bytes 524288 | tf_op jit(solution)/shard_map/all_to_all | solution.py:17
  35.6 47.9 %copy-start.4 = (s32[16,2]{0,1:T(2,128)S(1)}, s32[16,2]{0,1:T(2,128)}, u32[]{:S(2)}) copy-start(s32[16,2]{0,1:T(2,128)} %param.31) | copy-start | bytes 388
  35.6 54.7 %copy-start.3 = (bf16[256,256]{1,0:T(8,128)(2,1)S(1)}, bf16[256,256]{1,0:T(8,128)(2,1)}, u32[]{:S(2)}) copy-start(bf16[256,256]{1,0:T(8,128)(2,1)} %param.29) | copy-start | bytes 393220
  35.8 80.6 %copy-start.1 = (bf16[16,4096]{1,0:T(8,128)(2,1)S(1)}, bf16[16,4096]{1,0:T(8,128)(2,1)}, u32[]{:S(2)}) copy-start(bf16[16,4096]{1,0:T(8,128)(2,1)} %param.18) | copy-start | bytes 393220
  75.5 53.7 %copy-start.5 = (f32[16,2]{0,1:T(2,128)S(1)}, f32[16,2]{0,1:T(2,128)}, u32[]{:S(2)}) copy-start(f32[16,2]{0,1:T(2,128)} %param.32) | copy-start | bytes 388
  76.0 89.1 %copy-start.2 = (bf16[1,4096,128]{2,1,0:T(8,128)(2,1)S(1)}, bf16[1,4096,128]{2,1,0:T(8,128)(2,1)}, u32[]{:S(2)}) copy-start(bf16[1,4096,128]{2,1,0:T(8,128)(2,1)} %param.34) | copy-start | bytes 3145732
  80.0 10.3 %all-to-all-start.2 = ((bf16[16,16,256]{2,1,0:T(8,128)(2,1)}), bf16[16,16,256]{2,1,0:T(8,128)(2,1)S(1)}, u32[]{:S(2)}, u32[]{:S(2)}) async-start(bf16[16,16,256]{2,1,0:T(8,128)(2,1)} %broadcast_in_dim.22), calls=%async_computation.2 | async-start | bytes 262144 | tf_op jit(solution)/shard_map/all_to_all | solution.py:29
  91.2 11.0 %all-to-all-start.3 = ((bf16[16,16,256]{2,1,0:T(8,128)(2,1)}), bf16[16,16,256]{2,1,0:T(8,128)(2,1)}, u32[]{:S(2)}, u32[]{:S(2)}) async-start(bf16[16,16,256]{2,1,0:T(8,128)(2,1)} %bitcast.8), calls=%async_computation.3 | async-start | bytes 262144 | tf_op jit(solution)/shard_map/all_to_all | solution.py:119
  102.2 22.9 %all-to-all-start.4 = ((bf16[16,16,256]{2,1,0:T(8,128)(2,1)}), bf16[16,16,256]{2,1,0:T(8,128)(2,1)S(1)}, u32[]{:S(2)}, u32[]{:S(2)}) async-start(bf16[16,16,256]{2,1,0:T(8,128)(2,1)} %all-to-all-done.3), calls=%async_computation.4 | async-start | bytes 262144 | tf_op jit(solution)/shard_map/all_to_all | solution.py:17
  125.8 10.1 %all-to-all-start.5 = ((f32[16,1,16]{2,1,0:T(1,128)}), f32[16,1,16]{2,1,0:T(1,128)S(1)}, u32[]{:S(2)}, u32[]{:S(2)}) async-start(f32[16,1,16]{2,1,0:T(1,128)} %broadcast_in_dim.23), calls=%async_computation.5 | async-start | bytes 16384 | tf_op jit(solution)/shard_map/all_to_all | solution.py:29
  136.0 56.2 %copy-start.6 = (f32[128]{0:T(128)S(1)}, f32[128]{0:T(128)}, u32[]{:S(2)}) copy-start(f32[128]{0:T(128)} %param.24) | copy-start | bytes 1540
  166.6 21.4 %all-to-all-start.7 = ((bf16[16,64,256]{2,1,0:T(8,128)(2,1)}), bf16[16,64,256]{2,1,0:T(8,128)(2,1)S(1)}, u32[]{:S(2)}, u32[]{:S(2)}) async-start(bf16[16,64,256]{2,1,0:T(8,128)(2,1)} %bitcast.58), calls=%async_computation.7 | async-start | bytes 1048576 | tf_op jit(solution)/shard_map/all_to_all | solution.py:17
  188.6 9.9 %all-to-all-start.8 = ((bf16[16,4,256]{2,1,0:T(4,128)(2,1)}), bf16[16,4,256]{2,1,0:T(4,128)(2,1)S(1)}, u32[]{:S(2)}, u32[]{:S(2)}) async-start(bf16[16,4,256]{2,1,0:T(4,128)(2,1)} %all_to_all.67), calls=%async_computation.8 | async-start | bytes 65536 | tf_op jit(solution)/shard_map/all_to_all | solution.py:157
where the time goes:
time: 200 us; the launch traced here: 199 us
  waiting for transfers between devices  56.7 us (28%)
  other arithmetic  44.9 us (22%)
  blocking collectives  41.5 us (21%)
  starting transfers between devices  36.3 us (18%)
  matrix products  13.8 us (7%)
  local copies, waits for them, and re-layouts  5.17 us (3%)
    another operation x2, other arithmetic  39.7 us
    all_to_all x3, waiting for transfers between devices, sent_and_summed(): tiles = lax.all_to_all(split_up(shard, dim, size), axis, 0, 0, tiled=True)  32.3 us
    all_to_all x3, starting transfers between devices, sent_and_summed(): tiles = lax.all_to_all(split_up(shard, dim, size), axis, 0, 0, tiled=True)  21.7 us
    all_gather x1, blocking collectives, body(): arrived = lax.all_gather(moved, 'tp', axis=1, tiled=True)  18 us
    all_to_all x1, blocking collectives, body(): lax.all_to_all(normed, 'ep', split_axis=1, concat_axis=0, tiled=True)  14.2 us
    all_to_all x2, waiting for transfers between devices, sent_to_all(): lax.all_to_all(jnp.broadcast_to(shard[None], (size, *shard.shape)), axis,...  12.5 us
    all_to_all x1, blocking collectives, body(): lax.all_to_all(outgoing, 'ep', split_axis=0, concat_axis=0, tiled=True)  9.26 us
    all_to_all x2, starting transfers between devices, sent_to_all(): lax.all_to_all(jnp.broadcast_to(shard[None], (size, *shard.shape)), axis,...  6.88 us
  transfers between devices with their start and end apart: 7, of which 7 were waited for; matrix products, arithmetic and copies ran while one was open for 2% of the time, Pallas kernels for 0%

commit v1 on v0

v1 whole, which is shorter than its diff:
```python
import functools

import jax
import jax.numpy as jnp
from jax import lax
from jax.experimental import pallas as pl
from jax.experimental.pallas import tpu as pltpu
from jax.sharding import PartitionSpec as P

EPSILON = 1e-06
MESH = pl.DeviceIdType.MESH
F32 = jnp.float32
BF16 = jnp.bfloat16
ROWS = 16
CAP = 4


def iota(shape, dim):
    return lax.broadcasted_iota(jnp.int32, shape, dim)


def pieces(v):
    hi = v.astype(BF16)
    rest = v - hi.astype(F32)
    mid = rest.astype(BF16)
    low = (rest - mid.astype(F32)).astype(BF16)
    return hi, mid, low


def dot(a, b):
    return jnp.dot(a, b, preferred_element_type=F32)


def kernel(
    n,
    x_h,
    again,
    wq_h,
    wk_h,
    wv_h,
    qg,
    kg,
    ho,
    kc_h,
    vc_h,
    lens,
    wo_h,
    eg,
    routes,
    rw,
    gw_h,
    uw_h,
    dw_h,
    out,
    fk,
    fv,
    xv,
    xn,
    xg,
    wqkv,
    part,
    pr,
    kc,
    vc,
    att,
    agb,
    wo,
    terms,
    rsb,
    xts,
    xtr,
    res_s,
    res_r,
    disp,
    dx,
    xs,
    xa,
    wgu,
    acc,
    gu,
    hid,
    ha,
    dwr,
    ybuf,
    yt,
    rt,
    tri,
    pt,
    cmb,
    geb,
    quarter,
    lsem,
    ssem,
    rsem,
    dsem,
    drsem,
):
    e = lax.axis_index("ep")
    t = lax.axis_index("tp")
    width = n * 256
    cache = kc.shape[1]

    bar = pltpu.get_barrier_semaphore()

    def greet(d, c):
        pl.semaphore_signal(bar, inc=1, device_id=(lax.rem(e + d, n), t), device_id_type=MESH)
        pl.semaphore_signal(bar, inc=1, device_id=(e, lax.rem(t + d, n)), device_id_type=MESH)
        return c

    lax.fori_loop(1, n, greet, 0)

    def load(src, dst, k):
        cp = pltpu.make_async_copy(src, dst, lsem.at[k])
        cp.start()
        return cp

    lx = load(x_h, xv, 0)
    lq = load(wq_h, wqkv.at[:, pl.ds(0, 256)], 1)
    lk = load(wk_h, wqkv.at[:, pl.ds(256, 128)], 2)
    lv = load(wv_h, wqkv.at[:, pl.ds(384, 128)], 3)
    lo = load(wo_h, wo, 4)
    lkc = load(kc_h, kc, 5)
    lvc = load(vc_h, vc, 6)
    lg = load(gw_h.at[0], wgu.at[:, pl.ds(0, 128)], 7)
    lu = load(uw_h.at[0], wgu.at[:, pl.ds(128, 128)], 8)
    t256 = pl.multiple_of(t * 256, 256)
    ld = load(dw_h.at[0, :, pl.ds(t256, 256)], dwr.at[t], 9)

    def send(k, axis, src_at, dst):
        me = e if axis == "ep" else t

        def one(d, c):
            p = lax.rem(me + d, n)
            pltpu.make_async_remote_copy(
                src_ref=src_at(p),
                dst_ref=dst,
                send_sem=ssem.at[k],
                recv_sem=rsem.at[k],
                device_id=(p, t) if axis == "ep" else (e, p),
                device_id_type=MESH,
            ).start()
            return c

        lax.fori_loop(1, n, one, 0)

    def await_all(ref, sem):
        pltpu.make_async_copy(ref, ref, sem).wait()

    lx.wait()
    x = xv[...].astype(F32)
    meansq = jnp.sum(x * x, axis=1, keepdims=True) * (1.0 / width)
    xn[...] = (x * lax.rsqrt(meansq + EPSILON) * again[...]).astype(BF16)

    tri[...] = (iota((256, 256), 0) >= iota((256, 256), 1)).astype(F32).astype(BF16)
    lane = iota((ROWS, 8 * n), 1)
    lower = (iota((ROWS, ROWS), 0) > iota((ROWS, ROWS), 1)).astype(F32).astype(BF16)

    def placed_slots(first, second):
        member = jnp.where((first == lane // 8) | (second == lane // 8), 1.0, 0.0)
        rank = dot(lower, member.astype(BF16))
        return jnp.where(rank == (lane % 4).astype(F32), member, 0.0)

    r0 = routes[:, 0:1]
    r1 = routes[:, 1:2]
    slots = placed_slots(r0, r1)
    weighted = slots * jnp.where(r0 == lane // 8, rw[:, 0:1], rw[:, 1:2])
    first_half = jnp.where((lane // 4) % 2 == 0, weighted, 0.0)
    halves = jnp.concatenate([first_half, weighted - first_half], axis=0)
    c_hi, c_mid, c_low = pieces(halves)
    cmb[pl.ds(0, 2 * ROWS), :] = c_hi
    cmb[pl.ds(2 * ROWS, 2 * ROWS), :] = c_mid
    cmb[pl.ds(4 * ROWS, 2 * ROWS), :] = c_low
    for c in range(n):
        geb[c] = jnp.where(
            iota((8, 128), 0) < 4,
            jnp.broadcast_to(eg[2 * c : 2 * c + 1, :], (8, 128)),
            jnp.broadcast_to(eg[2 * c + 1 : 2 * c + 2, :], (8, 128)),
        )
    for s in range(4):
        quarter[s] = (iota((16, 128), 0) // 4 == s).astype(F32).astype(BF16)
    xts[:, pl.ds(0, 256)] = xv[:, pl.ds(t256, 256)].astype(F32)
    lanes = iota((ROWS, 128), 1)
    xts[:, pl.ds(256, 128)] = jnp.where(
        lanes == 0, r0.astype(F32), jnp.where(lanes == 1, r1.astype(F32), 0.0)
    )

    pl.semaphore_wait(bar, 2 * (n - 1))
    e16 = pl.multiple_of(e * ROWS, ROWS)
    e256 = pl.multiple_of(e * 256, 256)
    t16 = pl.multiple_of(t * ROWS, ROWS)
    send(0, "ep", lambda p: xn.at[:, pl.ds(pl.multiple_of(p * 256, 256), 256)], xg.at[pl.ds(e16, ROWS), :])
    xg[pl.ds(e16, ROWS), :] = xn[:, pl.ds(e256, 256)]

    def spread(d, c):
        p = lax.rem(t + d, n)
        pltpu.make_async_remote_copy(
            src_ref=dw_h.at[0, :, pl.ds(pl.multiple_of(p * 256, 256), 256)],
            dst_ref=dwr.at[t],
            send_sem=dsem,
            recv_sem=drsem,
            device_id=(e, p),
            device_id_type=MESH,
        ).start()
        return c

    lax.fori_loop(1, n, spread, 0)

    lq.wait()
    lk.wait()
    lv.wait()
    await_all(xg.at[pl.ds(0, (n - 1) * ROWS), :], rsem.at[0])

    def to_mirror(src, dst, k):
        return pltpu.make_async_remote_copy(
            src_ref=src,
            dst_ref=dst,
            send_sem=ssem.at[k],
            recv_sem=rsem.at[k],
            device_id=(t, e),
            device_id_type=MESH,
        )

    part[...] = dot(xg[...], wqkv[...]).astype(BF16)
    send(1, "ep", lambda p: part.at[pl.ds(pl.multiple_of(p * ROWS, ROWS), ROWS), :], pr.at[e])
    pr[e] = part[pl.ds(e16, ROWS), :]

    @pl.when(e != t)
    def _():
        to_mirror(xts, xtr, 8).start()

    @pl.when(e == t)
    def _():
        xtr[...] = xts[...]

    await_all(pr.at[pl.ds(0, n - 1)], rsem.at[1])
    summed = pr[0].astype(F32)
    for k in range(1, n):
        summed = summed + pr[k].astype(F32)

    def head_norm(raw, gain):
        v = raw.astype(BF16).astype(F32)
        meansq = jnp.sum(v * v, axis=1, keepdims=True) * (1.0 / 128)
        return v * lax.rsqrt(meansq + EPSILON) * gain

    fk[...] = head_norm(summed[:, 256:384], kg[...]).astype(BF16)
    fv[...] = summed[:, 384:512].astype(BF16)
    query = jnp.concatenate(
        [head_norm(summed[:, 0:128], qg[...]), head_norm(summed[:, 128:256], qg[...])], axis=0
    )
    row = iota((2 * ROWS, 128), 0)
    lkc.wait()
    z = jnp.zeros((2 * ROWS, cache), F32)
    for b in range(ROWS):
        own = jnp.where(row % ROWS == b, query, 0.0).astype(BF16)
        z = z + lax.dot_general(own, kc[b], (((1,), (1,)), ((), ())), preferred_element_type=F32)
    offset = jnp.where(iota((2 * ROWS, 1), 0) < ROWS, ho[0], ho[1])
    z = z * 128**-0.5 + offset
    lens_col = jnp.sum(
        jnp.where(
            iota((2 * ROWS, ROWS), 0) % ROWS == iota((2 * ROWS, ROWS), 1), lens[...].astype(F32), 0.0
        ),
        axis=1,
        keepdims=True,
    )
    live = iota((2 * ROWS, cache), 1).astype(F32) < lens_col
    breaks = jnp.where(live, jnp.maximum(z, 0.0) + jnp.log1p(jnp.exp(-jnp.abs(z))), 0.0)
    chunks = cache // 256
    parts = pieces(breaks)
    stacked = jnp.concatenate(
        [p[:, c * 256 : (c + 1) * 256] for p in parts for c in range(chunks)], axis=0
    )
    sums = dot(stacked, tri[...])
    size = chunks * 2 * ROWS
    sums = sums[:size] + sums[size : 2 * size] + sums[2 * size :]
    after = jnp.zeros((2 * ROWS, 1), F32)
    suffix = [None] * chunks
    for c in range(chunks - 1, -1, -1):
        here = sums[c * 2 * ROWS : (c + 1) * 2 * ROWS]
        suffix[c] = here + after
        after = after + here[:, 0:1]
    suffix = jnp.concatenate(suffix, axis=1)
    stick = jnp.where(live, jnp.exp(z - suffix), 0.0)
    lvc.wait()
    wide_row = iota((2 * ROWS, cache), 0)
    attended = jnp.zeros((2 * ROWS, 128), F32)
    for b in range(ROWS):
        own = jnp.where(wide_row % ROWS == b, stick, 0.0).astype(BF16)
        attended = attended + dot(own, vc[b])
    att[:, pl.ds(0, 128)] = attended[:ROWS].astype(BF16)
    att[:, pl.ds(128, 128)] = attended[ROWS:].astype(BF16)

    send(2, "ep", lambda p: att, agb.at[pl.ds(e16, ROWS), :])
    agb[pl.ds(e16, ROWS), :] = att[...]

    @pl.when(e != t)
    def _():
        to_mirror(xts, xtr, 8).wait_recv()

    theirs = placed_slots(xtr[:, 256:257].astype(jnp.int32), xtr[:, 257:258].astype(jnp.int32))
    pt[...] = jnp.transpose(theirs, (1, 0)).astype(BF16)

    lo.wait()
    await_all(agb.at[pl.ds(0, (n - 1) * ROWS), :], rsem.at[2])

    terms[...] = dot(agb[...], wo[...]).astype(BF16)
    send(3, "tp", lambda p: terms.at[pl.ds(pl.multiple_of(p * ROWS, ROWS), ROWS), :], rsb.at[t])
    rsb[t] = terms[pl.ds(t16, ROWS), :]
    await_all(rsb.at[pl.ds(0, n - 1)], rsem.at[3])
    projected = rsb[0].astype(F32)
    for k in range(1, n):
        projected = projected + rsb[k].astype(F32)
    residual = (xtr[:, pl.ds(0, 256)] + projected).astype(BF16)
    res_s[...] = residual

    picked = dot(pt[...], residual)
    disp[...] = jnp.where(
        (iota((8 * n, 128), 0) // 4) % 2 == 0, picked[:, 0:128], picked[:, 128:256]
    )
    send(4, "ep", lambda p: disp.at[pl.ds(pl.multiple_of(p * 8, 8), 8), :], dx.at[e])
    dx[e] = disp[pl.ds(pl.multiple_of(e * 8, 8), 8), :]

    @pl.when(e != t)
    def _():
        to_mirror(res_s, res_r, 9).start()

    @pl.when(e == t)
    def _():
        res_r[...] = res_s[...]

    await_all(dx.at[pl.ds(0, n - 1)], rsem.at[4])

    v = dx[...]
    squares = jnp.sum(jnp.sum(v * v, axis=0), axis=1, keepdims=True)
    squares = jnp.broadcast_to(squares, (8, 128))
    squares = squares + pltpu.roll(squares, 4, 0)
    scale = lax.rsqrt(squares * (1.0 / width) + EPSILON)
    xs[...] = (v * scale[None] * geb[...]).reshape(n // 2, 16, 128).astype(BF16)
    send(5, "tp", lambda p: xs, xa.at[t])
    xa[t] = xs[...]
    lg.wait()
    lu.wait()
    await_all(xa.at[pl.ds(0, n - 1)], rsem.at[5])

    total = jnp.zeros((n * 16, 256), F32)
    for c in range(n // 2):
        block = xa[:, c]
        lhs = jnp.concatenate(
            [(block * quarter[s][None]).reshape(n * 16, 128) for s in range(4)], axis=1
        )
        total = total + dot(lhs, wgu[pl.ds(c * 512, 512), :])
    acc[...] = total
    for b in range(n):
        gu[pl.ds(b * 4, 4), :] = (
            acc[pl.ds(b * 16, 4), :]
            + acc[pl.ds(b * 16 + 4, 4), :]
            + acc[pl.ds(b * 16 + 8, 4), :]
            + acc[pl.ds(b * 16 + 12, 4), :]
        )
    gate = gu[:, 0:128]
    hid[...] = (gate * jax.nn.sigmoid(gate) * gu[:, 128:256]).astype(BF16)

    send(6, "tp", lambda p: hid, ha.at[t])
    ha[t] = hid[...]
    ld.wait()
    await_all(dwr.at[pl.ds(0, n - 1)], drsem)
    await_all(ha.at[pl.ds(0, n - 1)], rsem.at[6])
    y = jnp.zeros((4 * n, 256), F32)
    for k in range(0, n, 2):
        lhs = jnp.concatenate([ha[k], ha[k + 1]], axis=1)
        y = y + dot(lhs, dwr[pl.ds(k, 2)].reshape(256, 256))
    ybuf[...] = y.astype(BF16).astype(F32)
    for b in range(n):
        yt[pl.ds(b * 8, 4), :] = ybuf[pl.ds(b * 4, 4), pl.ds(0, 128)]
        yt[pl.ds(b * 8 + 4, 4), :] = ybuf[pl.ds(b * 4, 4), pl.ds(128, 128)]

    send(7, "ep", lambda p: yt.at[pl.ds(pl.multiple_of(p * 8, 8), 8), :], rt.at[e])
    rt[e] = yt[pl.ds(pl.multiple_of(e * 8, 8), 8), :]

    @pl.when(e != t)
    def _():
        to_mirror(res_s, res_r, 9).wait_recv()

    await_all(rt.at[pl.ds(0, n - 1)], rsem.at[7])
    back = rt[...].reshape(8 * n, 128).astype(BF16)
    mixed = dot(cmb[...], back)
    mixed = mixed[0 : 2 * ROWS] + mixed[2 * ROWS : 4 * ROWS] + mixed[4 * ROWS :]
    mixed = jnp.concatenate([mixed[:ROWS], mixed[ROWS:]], axis=1)
    out[...] = (res_r[...].astype(F32) + mixed).astype(BF16)

    await_all(xg.at[pl.ds(0, (n - 1) * ROWS), :], ssem.at[0])
    await_all(pr.at[pl.ds(0, n - 1)], ssem.at[1])
    await_all(agb.at[pl.ds(0, (n - 1) * ROWS), :], ssem.at[2])
    await_all(rsb.at[pl.ds(0, n - 1)], ssem.at[3])
    await_all(dx.at[pl.ds(0, n - 1)], ssem.at[4])
    await_all(xa.at[pl.ds(0, n - 1)], ssem.at[5])
    await_all(ha.at[pl.ds(0, n - 1)], ssem.at[6])
    await_all(rt.at[pl.ds(0, n - 1)], ssem.at[7])
    await_all(dwr.at[pl.ds(0, n - 1)], dsem)

    @pl.when(e != t)
    def _():
        to_mirror(xts, xtr, 8).wait_send()
        to_mirror(res_s, res_r, 9).wait_send()


def body(
    hidden_in,
    attn_gain,
    query_weight,
    key_weight,
    value_weight,
    query_gain,
    key_gain,
    head_offset,
    key_cache,
    value_cache,
    lengths,
    out_weight,
    expert_gain,
    routes,
    route_weights,
    gate_weight,
    up_weight,
    down_weight,
):
    n = lax.axis_size("ep")
    width = hidden_in.shape[1]
    cache = key_cache.shape[1]
    vmem = pl.BlockSpec(memory_space=pltpu.VMEM)
    hbm = pl.BlockSpec(memory_space=pl.ANY)
    smem = pl.BlockSpec(memory_space=pltpu.SMEM)
    V = pltpu.VMEM
    scratch = [
        V((ROWS, width), BF16),
        V((ROWS, width), BF16),
        V((n * ROWS, 256), BF16),
        V((256, 512), BF16),
        V((n * ROWS, 512), BF16),
        V((n, ROWS, 512), BF16),
        V((ROWS, cache, 128), BF16),
        V((ROWS, cache, 128), BF16),
        V((ROWS, 256), BF16),
        V((n * ROWS, 256), BF16),
        V((256, 256), BF16),
        V((n * ROWS, 256), BF16),
        V((n, ROWS, 256), BF16),
        V((ROWS, 384), F32),
        V((ROWS, 384), F32),
        V((ROWS, 256), BF16),
        V((ROWS, 256), BF16),
        V((8 * n, 128), F32),
        V((n, 8, 128), F32),
        V((n // 2, 16, 128), BF16),
        V((n, n // 2, 16, 128), BF16),
        V((width, 256), BF16),
        V((n * 16, 256), F32),
        V((n * 4, 256), F32),
        V((n * 4, 128), BF16),
        V((n, n * 4, 128), BF16),
        V((n, 128, 256), BF16),
        V((n * 4, 256), F32),
        V((8 * n, 128), F32),
        V((n, 8, 128), F32),
        V((256, 256), BF16),
        V((8 * n, ROWS), BF16),
        V((6 * ROWS, 8 * n), BF16),
        V((n, 8, 128), F32),
        V((4, 16, 128), BF16),
        pltpu.SemaphoreType.DMA((10,)),
        pltpu.SemaphoreType.DMA((10,)),
        pltpu.SemaphoreType.DMA((10,)),
        pltpu.SemaphoreType.DMA,
        pltpu.SemaphoreType.DMA,
    ]
    return pl.pallas_call(
        functools.partial(kernel, n),
        out_shape=(
            jax.ShapeDtypeStruct((ROWS, 256), BF16),
            jax.ShapeDtypeStruct((ROWS, 128), BF16),
            jax.ShapeDtypeStruct((ROWS, 128), BF16),
        ),
        in_specs=[hbm, vmem, hbm, hbm, hbm, vmem, vmem, smem, hbm, hbm, vmem, hbm]
        + [vmem, vmem, vmem, hbm, hbm, hbm],
        out_specs=(vmem, vmem, vmem),
        scratch_shapes=scratch,
        compiler_params=pltpu.CompilerParams(
            collective_id=0, has_side_effects=True, vmem_limit_bytes=60 * 1024 * 1024
        ),
    )(
        hidden_in,
        attn_gain.reshape(1, width),
        query_weight,
        key_weight,
        value_weight,
        query_gain.reshape(1, 128),
        key_gain.reshape(1, 128),
        head_offset,
        key_cache,
        value_cache,
        lengths.reshape(1, ROWS),
        out_weight,
        expert_gain.reshape(width // 128, 128),
        routes,
        route_weights,
        gate_weight,
        up_weight,
        down_weight,
    )


def solution(mesh):
    placed = (
        P("ep", None),
        P(),
        P("ep", "tp"),
        P("ep", "tp"),
        P("ep", "tp"),
        P(),
        P(),
        P("tp"),
        P("ep", None, "tp"),
        P("ep", None, "tp"),
        P("ep"),
        P("tp", "ep"),
        P(),
        P("ep", None),
        P("ep", None),
        P("ep", None, "tp"),
        P("ep", None, "tp"),
        P("ep", "tp", None),
    )
    return jax.shard_map(
        body,
        mesh=mesh,
        in_specs=placed,
        out_specs=(P("ep", "tp"), P("ep", "tp"), P("ep", "tp")),
        check_vma=False,
    )
```

time: 200 us -> 88.1 us (0.44)
  Pallas kernels: 0 us -> 80.6 us
  waiting for transfers between devices: 56.7 us -> 0 us
  other arithmetic: 44.9 us -> 0 us
  blocking collectives: 41.5 us -> 0 us
  starting transfers between devices: 36.3 us -> 0 us
  matrix products: 13.8 us -> 0 us
    pallas_call x0 -> x1, Pallas kernels: none -> 80.6 us  [body(): pl.pallas_call(functools.partial(kernel, n), out_shape=(jax.ShapeDtypeStr...]
    all_to_all x7 -> x0, waiting for transfers between devices: 56.7 us -> none  [the longest x3 32.3 us: sent_and_summed(): tiles = lax.all_to_all(split_up(shard, dim, size), axis, 0, 0, tiled=True)]
    another operation x3 -> x0, other arithmetic: 39.7 us -> none
    all_to_all x7 -> x0, starting transfers between devices: 36.3 us -> none  [the longest x3 21.7 us: sent_and_summed(): tiles = lax.all_to_all(split_up(shard, dim, size), axis, 0, 0, tiled=True)]
    all_to_all x2 -> x0, blocking collectives: 23.5 us -> none  [the longest x1 14.2 us: body(): lax.all_to_all(normed, 'ep', split_axis=1, concat_axis=0, tiled=True)]
    all_gather x1 -> x0, blocking collectives: 18 us -> none  [body(): arrived = lax.all_gather(moved, 'tp', axis=1, tiled=True)]
    dot_general x10 -> x0, matrix products: 13.8 us -> none  [the longest x1 3.45 us: body(): jnp.einsum('bkgd,bskd->bkgs', grouped, cached_keys, preferred_element_typ...]
    unnamed x16 -> x5, local copies, waits for them, and re-layouts: 0.14 us -> 6.53 us
  transfers between devices with their start and end apart: 7 -> 0, of which waited for: 7 -> 0; matrix products, arithmetic and copies ran while one was open for 2% -> 0% of each run, Pallas kernels for 0% -> 0%
where the time goes in v1:
time: 88.1 us; the launch traced here: 87.8 us
  Pallas kernels  80.6 us (91%)
  local copies, waits for them, and re-layouts  6.53 us (7%)
    pallas_call x1, Pallas kernels, body(): pl.pallas_call(functools.partial(kernel, n), out_shape=(jax.ShapeDtypeStr...  80.6 us
    unnamed x5, local copies, waits for them, and re-layouts  6.53 us

profile of v1, /device:TPU:1, one launch (start us, length us, event | category | flops | bytes accessed | tf_op | source)
XLA Modules:
  0.0 87.8 jit_solution(14365638137495760186)
XLA Ops:
  0.6 1.4 %copy.21.routes = s32[16,2]{1,0:T(8,128)} copy(s32[16,2]{0,1:T(2,128)} %param.31) | data formatting | bytes 256 | tf_op args[13]
  2.0 1.3 %copy.22.rw = f32[16,2]{1,0:T(8,128)} copy(f32[16,2]{0,1:T(2,128)} %param.32) | data formatting | bytes 256 | tf_op args[14]
  3.3 80.6 %shard_map.193 = (bf16[16,256]{1,0:T(8,128)(2,1)}, bf16[16,128]{1,0:T(8,128)(2,1)}, bf16[16,128]{1,0:T(8,128)(2,1)}) custom-call(bf16[16,4096]{1,0:T(8,128)(2,1)} %x_h.1, f32[1,4096]{1,0:T(1,128)} %bitcast.5, bf16[256,256]{1,0:T(8,128)(2,1)} %wq_h.1, bf16[256,128]{1,0:T(8,128)(2,1)} %wk_h.1, bf16[256,128]{1,0:T(8,128)(2,1)} %wv_h.1, f32[1,128]{1,0:T(1,128)} %bitcast.7, ...), custom_call_target="tpu_custom_call" | custom-call | tf_op jit(solution)/shard_map/pallas_call | solution.py:475
  83.9 1.3 %copy.26 = bf16[16,256]{1,0:T(8,128)(2,1)} copy(bf16[16,256]{1,0:T(8,128)(2,1)} %get-tuple-element.6) | data formatting | bytes 16384
  85.2 1.3 %copy.27 = bf16[16,128]{1,0:T(8,128)(2,1)} copy(bf16[16,128]{1,0:T(8,128)(2,1)} %get-tuple-element.7) | data formatting | bytes 8192
  86.5 1.3 %copy.28 = bf16[16,128]{1,0:T(8,128)(2,1)} copy(bf16[16,128]{1,0:T(8,128)(2,1)} %get-tuple-element.8) | data formatting | bytes 8192

commit v2 on v1

v2 whole, which is shorter than its diff:
```python
import functools
import math

import jax
import jax.numpy as jnp
from jax import lax
from jax.experimental import pallas as pl
from jax.experimental.pallas import tpu as pltpu
from jax.sharding import PartitionSpec as P

EPSILON = 1e-06
MESH = pl.DeviceIdType.MESH
F32 = jnp.float32
BF16 = jnp.bfloat16
ROWS = 16
CAP = 4


def iota(shape, dim):
    return lax.broadcasted_iota(jnp.int32, shape, dim)


def pieces(v):
    hi = v.astype(BF16)
    rest = v - hi.astype(F32)
    mid = rest.astype(BF16)
    low = (rest - mid.astype(F32)).astype(BF16)
    return hi, mid, low


def dot(a, b):
    return jnp.dot(a, b, preferred_element_type=F32)


def plane_steps(n):
    side = math.isqrt(n)
    steps = [(dy, dx) for dy in range(side) for dx in range(side) if (dy, dx) != (0, 0)]
    return sorted(steps, key=lambda s: -sum(min(d, side - d) for d in s))


def column_steps(n):
    deep = n // 2
    steps = [(dz, dc) for dz in range(deep) for dc in range(2) if (dz, dc) != (0, 0)]
    return sorted(steps, key=lambda s: -min(s[0], deep - s[0]))


def kernel(
    n,
    x_h,
    again_h,
    wq_h,
    wk_h,
    wv_h,
    qg_h,
    kg_h,
    ho_h,
    kc_h,
    vc_h,
    lens_h,
    wo_h,
    eg_h,
    routes_h,
    rw_h,
    gw_h,
    uw_h,
    dw_h,
    out,
    fk,
    fv,
    again,
    qg,
    kg,
    ho,
    lens,
    eg,
    routes,
    rw,
    xv,
    xn,
    xg,
    wqkv,
    partq,
    partk,
    prq,
    prk,
    kc,
    vc,
    att,
    agb,
    wo,
    terms,
    rsb,
    xts,
    xtr,
    res_s,
    res_r,
    disp,
    xd,
    wgu,
    dwp,
    ys,
    rt,
    tri,
    pt,
    cmb,
    geb,
    lsem,
    ssem,
    rsem,
    bsend,
    brecv,
):
    e = lax.axis_index("ep")
    t = lax.axis_index("tp")
    side = math.isqrt(n)
    deep = n // 2
    ey, ex = e // side, lax.rem(e, side)
    tz, core = t // 2, lax.rem(t, 2)
    width = n * 256
    cache = kc.shape[1]

    def in_plane(step):
        return lax.rem(ey + step[0], side) * side + lax.rem(ex + step[1], side)

    def in_column(step):
        return lax.rem(tz + step[0], deep) * 2 + lax.rem(core + step[1], 2)

    bar = pltpu.get_barrier_semaphore()
    for step in plane_steps(n):
        pl.semaphore_signal(bar, inc=1, device_id=(in_plane(step), t), device_id_type=MESH)
    for step in column_steps(n):
        pl.semaphore_signal(bar, inc=1, device_id=(e, in_column(step)), device_id_type=MESH)

    def load(src, dst, k):
        cp = pltpu.make_async_copy(src, dst, lsem.at[k])
        cp.start()
        return cp

    mine256 = pl.multiple_of(core * 256, 128)
    lx = load(x_h, xv, 0)
    small = [load(a, b, 11 + i) for i, (a, b) in enumerate([(again_h, again), (qg_h, qg), (kg_h, kg), (ho_h, ho), (lens_h, lens), (eg_h, eg), (routes_h, routes), (rw_h, rw)])]
    lq = load(wq_h, wqkv.at[:, pl.ds(0, 256)], 1)
    lk = load(wk_h, wqkv.at[:, pl.ds(256, 128)], 2)
    lv = load(wv_h, wqkv.at[:, pl.ds(384, 128)], 3)
    lo = load(wo_h, wo, 4)
    lkc = load(kc_h, kc, 5)
    lvc = load(vc_h, vc, 6)
    lg = load(gw_h.at[0], wgu.at[:, pl.ds(mine256, 128)], 7)
    lu = load(uw_h.at[0], wgu.at[:, pl.ds(pl.multiple_of(mine256 + 128, 128), 128)], 8)
    ld = load(dw_h.at[0], dwp.at[core], 9)

    def remote(src, dst, k, dev, s=ssem, r=rsem):
        return pltpu.make_async_remote_copy(
            src_ref=src,
            dst_ref=dst,
            send_sem=s.at[k],
            recv_sem=r.at[k],
            device_id=dev,
            device_id_type=MESH,
        )

    def rows_of(p, size=ROWS):
        return pl.ds(pl.multiple_of(p * size, size), size)

    def cols_of(p, size=256):
        return pl.ds(pl.multiple_of(p * size, size), size)

    def await_all(ref, sem):
        pltpu.make_async_copy(ref, ref, sem).wait()

    lx.wait()
    for cp in small:
        cp.wait()
    x = xv[...].astype(F32)
    meansq = jnp.sum(x * x, axis=1, keepdims=True) * (1.0 / width)
    xn[...] = (x * lax.rsqrt(meansq + EPSILON) * again[...]).astype(BF16)

    tri[...] = (iota((256, 256), 0) >= iota((256, 256), 1)).astype(F32).astype(BF16)
    lane = iota((ROWS, 8 * n), 1)
    lower = (iota((ROWS, ROWS), 0) > iota((ROWS, ROWS), 1)).astype(F32).astype(BF16)
    diagonal = iota((ROWS, ROWS), 0) == iota((ROWS, ROWS), 1)

    def column(line):
        return jnp.sum(jnp.where(diagonal, line, 0.0), axis=1, keepdims=True)

    expert = (lane // 8).astype(F32)

    def placed_slots(first, second):
        member = jnp.where((first == expert) | (second == expert), 1.0, 0.0)
        rank = dot(lower, member.astype(BF16))
        return jnp.where(rank == (lane % 4).astype(F32), member, 0.0)

    r0 = column(routes[0:1, :].astype(F32))
    r1 = column(routes[1:2, :].astype(F32))
    slots = placed_slots(r0, r1)
    weighted = slots * jnp.where(r0 == expert, column(rw[0:1, :]), column(rw[1:2, :]))
    first_half = jnp.where((lane // 4) % 2 == 0, weighted, 0.0)
    halves = jnp.concatenate([first_half, weighted - first_half], axis=0)
    c_hi, c_mid, c_low = pieces(halves)
    cmb[pl.ds(0, 2 * ROWS), :] = c_hi
    cmb[pl.ds(2 * ROWS, 2 * ROWS), :] = c_mid
    cmb[pl.ds(4 * ROWS, 2 * ROWS), :] = c_low
    for c in range(n):
        geb[c] = jnp.where(
            iota((8, 128), 0) < 4,
            jnp.broadcast_to(eg[2 * c : 2 * c + 1, :], (8, 128)),
            jnp.broadcast_to(eg[2 * c + 1 : 2 * c + 2, :], (8, 128)),
        )
    xts[:, pl.ds(0, 256)] = xv[:, cols_of(t)].astype(F32)
    lanes = iota((ROWS, 128), 1)
    xts[:, pl.ds(256, 128)] = jnp.where(lanes == 0, r0, jnp.where(lanes == 1, r1, 0.0))

    pl.semaphore_wait(bar, 2 * (n - 1))
    for step in plane_steps(n):
        p = in_plane(step)
        remote(xn.at[:, cols_of(p)], xg.at[rows_of(e), :], 0, (p, t)).start()
    xg[rows_of(e), :] = xn[:, cols_of(e)]
    lq.wait()
    lk.wait()
    lv.wait()
    others = pl.ds(0, n - 1)
    other_rows = pl.ds(0, (n - 1) * ROWS)
    await_all(xg.at[other_rows, :], rsem.at[0])

    partq[...] = dot(xg[...], wqkv[:, pl.ds(0, 256)]).astype(BF16)
    for step in plane_steps(n):
        p = in_plane(step)
        remote(partq.at[rows_of(p), :], prq.at[e], 1, (p, t)).start()
    prq[e] = partq[rows_of(e), :]
    partk[...] = dot(xg[...], wqkv[:, pl.ds(256, 256)]).astype(BF16)
    for step in plane_steps(n):
        p = in_plane(step)
        remote(partk.at[rows_of(p), :], prk.at[e], 2, (p, t)).start()
    prk[e] = partk[rows_of(e), :]

    @pl.when(e != t)
    def _():
        remote(xts, xtr, 3, (t, e)).start()

    @pl.when(e == t)
    def _():
        xtr[...] = xts[...]

    def head_norm(raw, gain):
        v = raw.astype(BF16).astype(F32)
        meansq = jnp.sum(v * v, axis=1, keepdims=True) * (1.0 / 128)
        return v * lax.rsqrt(meansq + EPSILON) * gain

    def added(ref):
        total = ref[0].astype(F32)
        for k in range(1, n):
            total = total + ref[k].astype(F32)
        return total

    await_all(prq.at[others], rsem.at[1])

    other = (e, tz * 2 + 1 - core)
    swaps = [
        remote(gw_h.at[0], wgu.at[:, pl.ds(mine256, 128)], 0, other, bsend, brecv),
        remote(
            uw_h.at[0],
            wgu.at[:, pl.ds(pl.multiple_of(mine256 + 128, 128), 128)],
            1,
            other,
            bsend,
            brecv,
        ),
        remote(dw_h.at[0], dwp.at[core], 2, other, bsend, brecv),
    ]
    for cp in swaps:
        cp.start()

    summed = added(prq)
    query = jnp.concatenate(
        [head_norm(summed[:, 0:128], qg[...]), head_norm(summed[:, 128:256], qg[...])], axis=0
    )
    row = iota((2 * ROWS, 128), 0)
    lkc.wait()
    z = jnp.zeros((2 * ROWS, cache), F32)
    for b in range(ROWS):
        own = jnp.where(row % ROWS == b, query, 0.0).astype(BF16)
        z = z + lax.dot_general(own, kc[b], (((1,), (1,)), ((), ())), preferred_element_type=F32)
    offset = jnp.where(iota((2 * ROWS, 1), 0) < ROWS, ho[0:1, 0:1], ho[0:1, 1:2])
    z = z * 128**-0.5 + offset
    lens_col = jnp.sum(
        jnp.where(
            iota((2 * ROWS, ROWS), 0) % ROWS == iota((2 * ROWS, ROWS), 1), lens[...].astype(F32), 0.0
        ),
        axis=1,
        keepdims=True,
    )
    live = iota((2 * ROWS, cache), 1).astype(F32) < lens_col
    breaks = jnp.where(live, jnp.maximum(z, 0.0) + jnp.log1p(jnp.exp(-jnp.abs(z))), 0.0)
    chunks = cache // 256
    parts = pieces(breaks)
    stacked = jnp.concatenate(
        [p[:, c * 256 : (c + 1) * 256] for p in parts for c in range(chunks)], axis=0
    )
    sums = dot(stacked, tri[...])
    size = chunks * 2 * ROWS
    sums = sums[:size] + sums[size : 2 * size] + sums[2 * size :]
    after = jnp.zeros((2 * ROWS, 1), F32)
    suffix = [None] * chunks
    for c in range(chunks - 1, -1, -1):
        here = sums[c * 2 * ROWS : (c + 1) * 2 * ROWS]
        suffix[c] = here + after
        after = after + here[:, 0:1]
    suffix = jnp.concatenate(suffix, axis=1)
    stick = jnp.where(live, jnp.exp(z - suffix), 0.0)
    lvc.wait()
    wide_row = iota((2 * ROWS, cache), 0)
    attended = jnp.zeros((2 * ROWS, 128), F32)
    for b in range(ROWS):
        own = jnp.where(wide_row % ROWS == b, stick, 0.0).astype(BF16)
        attended = attended + dot(own, vc[b])
    att[:, pl.ds(0, 128)] = attended[:ROWS].astype(BF16)
    att[:, pl.ds(128, 128)] = attended[ROWS:].astype(BF16)

    for step in plane_steps(n):
        remote(att, agb.at[rows_of(e), :], 4, (in_plane(step), t)).start()
    agb[rows_of(e), :] = att[...]

    await_all(prk.at[others], rsem.at[2])
    summed = added(prk)
    fk[...] = head_norm(summed[:, 0:128], kg[...]).astype(BF16)
    fv[...] = summed[:, 128:256].astype(BF16)

    @pl.when(e != t)
    def _():
        remote(xts, xtr, 3, (t, e)).wait_recv()

    theirs = placed_slots(xtr[:, 256:257], xtr[:, 257:258])
    pt[...] = jnp.transpose(theirs, (1, 0)).astype(BF16)

    lo.wait()
    await_all(agb.at[other_rows, :], rsem.at[4])

    terms[...] = dot(agb[...], wo[...]).astype(BF16)
    for step in column_steps(n):
        p = in_column(step)
        remote(terms.at[rows_of(p), :], rsb.at[t], 5, (e, p)).start()
    rsb[t] = terms[rows_of(t), :]
    await_all(rsb.at[others], rsem.at[5])
    residual = (xtr[:, pl.ds(0, 256)] + added(rsb)).astype(BF16)
    res_s[...] = residual

    picked = dot(pt[...], residual)
    half = (iota((8 * n, 128), 0) // 4) % 2
    disp[...] = (
        jnp.where(half == 0, picked[:, 0:128], picked[:, 128:256]).reshape(n, 8, 128).astype(BF16)
    )

    def dispatch(dz):
        there = lax.rem(tz + dz, deep) * 2 + core
        for step in plane_steps(n):
            p = in_plane(step)
            remote(disp.at[p], xd.at[tz * n + e], 6, (p, there)).start()
        return there

    def dispatch_far(i, c):
        there = dispatch(deep // 2 + (i + 1) // 2 * (2 * lax.rem(i, 2) - 1))
        remote(disp.at[e], xd.at[tz * n + e], 6, (e, there)).start()
        return c

    lax.fori_loop(0, deep - 1, dispatch_far, 0)
    dispatch(0)
    xd[tz * n + e] = disp[e]

    @pl.when(e != t)
    def _():
        remote(res_s, res_r, 7, (t, e)).start()

    @pl.when(e == t)
    def _():
        res_r[...] = res_s[...]

    lg.wait()
    lu.wait()
    swaps[0].wait_recv()
    swaps[1].wait_recv()

    all_but_one = pl.ds(0, deep * n - 1)
    await_all(xd.at[all_but_one], rsem.at[6])

    squares = jnp.zeros((deep, 8, 128), F32)
    arrived = xd[...].reshape(deep, n, 8, 128)
    for c in range(n):
        v = arrived[:, c].astype(F32)
        squares = squares + v * v
    squares = jnp.sum(squares, axis=2, keepdims=True)
    squares = jnp.broadcast_to(squares, (deep, 8, 128)).reshape(deep * 8, 128)

    def both_halves(v):
        return jnp.concatenate(
            [v[i * 8 : i * 8 + 8] + pltpu.roll(v[i * 8 : i * 8 + 8], 4, 0) for i in range(deep)], axis=0
        )

    scale = lax.rsqrt(both_halves(squares) * (1.0 / width) + EPSILON)
    first = (iota((deep * 8, 128), 0) // 4) % 2 == 0
    total = jnp.zeros((deep * 8, 512), F32)
    for c in range(n):
        v = (arrived[:, c].astype(F32) * geb[c][None]).reshape(deep * 8, 128)
        v = v * scale
        lhs = jnp.concatenate([jnp.where(first, v, 0.0), jnp.where(first, 0.0, v)], axis=1)
        total = total + dot(lhs.astype(BF16), wgu[pl.ds(c * 256, 256), :])
    total = both_halves(total)
    hidden = []
    for k in range(2):
        gate = total[:, k * 256 : k * 256 + 128]
        hidden.append(gate * jax.nn.sigmoid(gate) * total[:, k * 256 + 128 : k * 256 + 256])
    hidden = jnp.concatenate(hidden, axis=1)
    wide_first = (iota((deep * 8, 256), 0) // 4) % 2 == 0
    hidden0 = jnp.where(wide_first, hidden, 0.0).astype(BF16)
    hidden1 = jnp.where(wide_first, 0.0, hidden).astype(BF16)
    ld.wait()
    swaps[2].wait_recv()
    down = dwp[...].reshape(256, width)
    for c in range(n):
        y = dot(hidden0, down[:, c * 256 : c * 256 + 128]) + dot(
            hidden1, down[:, c * 256 + 128 : c * 256 + 256]
        )
        ys[:, c] = y.reshape(deep, 8, 128).astype(BF16)

    def give_back(dz, dc, skip):
        there = lax.rem(tz + dz, deep) * 2 + lax.rem(core + dc, 2)
        for i in range(deep):
            b = 2 * i + core
            cp = remote(ys.at[i, there], rt.at[tz * n + e], 8, (b, there))
            if not skip:
                cp.start()
                continue

            @pl.when(b != e)
            def _():
                cp.start()

            @pl.when(b == e)
            def _():
                rt[tz * n + e] = ys[i, there]

    def give_far(i, c):
        dz = deep // 2 + (i + 1) // 2 * (2 * lax.rem(i, 2) - 1)
        give_back(dz, 0, False)
        give_back(dz, 1, False)
        return c

    lax.fori_loop(0, deep - 1, give_far, 0)
    give_back(0, 1, False)
    give_back(0, 0, True)

    @pl.when(e != t)
    def _():
        remote(res_s, res_r, 7, (t, e)).wait_recv()

    def await_returned(sem):
        @pl.when(lax.rem(e, 2) != core)
        def _():
            await_all(rt, sem)

        @pl.when(lax.rem(e, 2) == core)
        def _():
            await_all(rt.at[all_but_one], sem)

    await_returned(rsem.at[8])
    back = rt[pl.ds(0, n)].astype(F32)
    for k in range(1, deep):
        back = back + rt[pl.ds(k * n, n)].astype(F32)
    mixed = dot(cmb[...], back.reshape(8 * n, 128).astype(BF16))
    mixed = mixed[0 : 2 * ROWS] + mixed[2 * ROWS : 4 * ROWS] + mixed[4 * ROWS :]
    mixed = jnp.concatenate([mixed[:ROWS], mixed[ROWS:]], axis=1)
    out[...] = (res_r[...].astype(F32) + mixed).astype(BF16)

    await_all(xg.at[other_rows, :], ssem.at[0])
    await_all(prq.at[others], ssem.at[1])
    await_all(prk.at[others], ssem.at[2])
    await_all(agb.at[other_rows, :], ssem.at[4])
    await_all(rsb.at[others], ssem.at[5])
    await_all(xd.at[all_but_one], ssem.at[6])
    await_returned(ssem.at[8])
    for cp in swaps:
        cp.wait_send()

    @pl.when(e != t)
    def _():
        remote(xts, xtr, 3, (t, e)).wait_send()
        remote(res_s, res_r, 7, (t, e)).wait_send()


def emit(a, b, c, a_out, b_out, c_out):
    a_out[...] = a[...]
    b_out[...] = b[...]
    c_out[...] = c[...]


def body(
    hidden_in,
    attn_gain,
    query_weight,
    key_weight,
    value_weight,
    query_gain,
    key_gain,
    head_offset,
    key_cache,
    value_cache,
    lengths,
    out_weight,
    expert_gain,
    routes,
    route_weights,
    gate_weight,
    up_weight,
    down_weight,
):
    n = lax.axis_size("ep")
    width = hidden_in.shape[1]
    cache = key_cache.shape[1]
    vmem = pl.BlockSpec(memory_space=pltpu.VMEM)
    hbm = pl.BlockSpec(memory_space=pl.ANY)
    V = pltpu.VMEM
    I32 = jnp.int32
    deep = n // 2
    scratch = [
        V((1, width), F32),
        V((1, 128), F32),
        V((1, 128), F32),
        V((1, 2), F32),
        V((1, ROWS), I32),
        V((width // 128, 128), F32),
        V((2, ROWS), I32),
        V((2, ROWS), F32),
        V((ROWS, width), BF16),
        V((ROWS, width), BF16),
        V((n * ROWS, 256), BF16),
        V((256, 512), BF16),
        V((n * ROWS, 256), BF16),
        V((n * ROWS, 256), BF16),
        V((n, ROWS, 256), BF16),
        V((n, ROWS, 256), BF16),
        V((ROWS, cache, 128), BF16),
        V((ROWS, cache, 128), BF16),
        V((ROWS, 256), BF16),
        V((n * ROWS, 256), BF16),
        V((256, 256), BF16),
        V((n * ROWS, 256), BF16),
        V((n, ROWS, 256), BF16),
        V((ROWS, 384), F32),
        V((ROWS, 384), F32),
        V((ROWS, 256), BF16),
        V((ROWS, 256), BF16),
        V((n, 8, 128), BF16),
        V((deep * n, 8, 128), BF16),
        V((width, 512), BF16),
        V((2, 128, width), BF16),
        V((deep, n, 8, 128), BF16),
        V((deep * n, 8, 128), BF16),
        V((256, 256), BF16),
        V((8 * n, ROWS), BF16),
        V((6 * ROWS, 8 * n), BF16),
        V((n, 8, 128), F32),
        pltpu.SemaphoreType.DMA((20,)),
        pltpu.SemaphoreType.DMA((9,)),
        pltpu.SemaphoreType.DMA((9,)),
        pltpu.SemaphoreType.DMA((3,)),
        pltpu.SemaphoreType.DMA((3,)),
    ]
    results = (
        jax.ShapeDtypeStruct((ROWS, 256), BF16),
        jax.ShapeDtypeStruct((ROWS, 128), BF16),
        jax.ShapeDtypeStruct((ROWS, 128), BF16),
    )
    made = pl.pallas_call(
        functools.partial(kernel, n),
        out_shape=results,
        in_specs=[hbm] * 18,
        out_specs=(vmem, vmem, vmem),
        scratch_shapes=scratch,
        compiler_params=pltpu.CompilerParams(
            collective_id=0, has_side_effects=True, vmem_limit_bytes=60 * 1024 * 1024
        ),
    )(
        hidden_in,
        attn_gain.reshape(1, width),
        query_weight,
        key_weight,
        value_weight,
        query_gain.reshape(1, 128),
        key_gain.reshape(1, 128),
        head_offset.reshape(1, 2),
        key_cache,
        value_cache,
        lengths.reshape(1, ROWS),
        out_weight,
        expert_gain.reshape(width // 128, 128),
        routes.T,
        route_weights.T,
        gate_weight,
        up_weight,
        down_weight,
    )
    return pl.pallas_call(
        emit, out_shape=results, in_specs=[vmem] * 3, out_specs=(vmem, vmem, vmem)
    )(*made)


def solution(mesh):
    placed = (
        P("ep", None),
        P(),
        P("ep", "tp"),
        P("ep", "tp"),
        P("ep", "tp"),
        P(),
        P(),
        P("tp"),
        P("ep", None, "tp"),
        P("ep", None, "tp"),
        P("ep"),
        P("tp", "ep"),
        P(),
        P("ep", None),
        P("ep", None),
        P("ep", None, "tp"),
        P("ep", None, "tp"),
        P("ep", "tp", None),
    )
    return jax.shard_map(
        body,
        mesh=mesh,
        in_specs=placed,
        out_specs=(P("ep", "tp"), P("ep", "tp"), P("ep", "tp")),
        check_vma=False,
    )
```

time: 88.1 us -> 59.7 us (0.68)
  Pallas kernels: 80.6 us -> 58.9 us
  local copies, waits for them, and re-layouts: 6.53 us -> 0 us
    pallas_call x1 -> x2, Pallas kernels: 80.6 us -> 58.9 us  [the longest x1 57.6 us: body(): pl.pallas_call(functools.partial(kernel, n), out_shape=results, in_specs=...]
    unnamed x5 -> x0, local copies, waits for them, and re-layouts: 6.53 us -> none
where the time goes in v2:
time: 59.7 us; the launch traced here: 59.6 us
  Pallas kernels  58.9 us (99%)
  between operations  0.65 us (1%)
    pallas_call x1, Pallas kernels, body(): pl.pallas_call(functools.partial(kernel, n), out_shape=results, in_specs=...  57.6 us
    pallas_call x1, Pallas kernels, body(): pl.pallas_call(emit, out_shape=results, in_specs=[vmem] * 3, out_specs=(v...  1.31 us

profile of v2, /device:TPU:1, one launch (start us, length us, event | category | flops | bytes accessed | tf_op | source)
XLA Modules:
  0.0 59.6 jit_solution(15167552910625897544)
XLA Ops:
  0.6 57.6 %shard_map.193 = (bf16[16,256]{1,0:T(8,128)(2,1)}, bf16[16,128]{1,0:T(8,128)(2,1)}, bf16[16,128]{1,0:T(8,128)(2,1)}) custom-call(bf16[16,4096]{1,0:T(8,128)(2,1)} %x_h.1, f32[1,4096]{1,0:T(1,128)} %bitcast.8, bf16[256,256]{1,0:T(8,128)(2,1)} %wq_h.1, bf16[256,128]{1,0:T(8,128)(2,1)} %wk_h.1, bf16[256,128]{1,0:T(8,128)(2,1)} %wv_h.1, f32[1,128]{1,0:T(1,128)} %bitcast.12, ...), custom_call_target="tpu_custom_call" | custom-call | tf_op jit(solution)/shard_map/pallas_call | solution.py:572
  58.3 1.3 %shard_map.194 = (bf16[16,256]{1,0:T(8,128)(2,1)}, bf16[16,128]{1,0:T(8,128)(2,1)}, bf16[16,128]{1,0:T(8,128)(2,1)}) custom-call(bf16[16,256]{1,0:T(8,128)(2,1)} %get-tuple-element.6.a, bf16[16,128]{1,0:T(8,128)(2,1)} %get-tuple-element.7.b, bf16[16,128]{1,0:T(8,128)(2,1)} %get-tuple-element.8.c), custom_call_target="tpu_custom_call" | custom-call | tf_op jit(solution)/shard_map/pallas_call | solution.py:601

commit v3 on v2

--- a/solution.py
+++ b/solution.py
@@ -122,6 +122,18 @@
     def in_plane(step):
         return lax.rem(ey + step[0], side) * side + lax.rem(ex + step[1], side)
 
+    shift = lax.rem(core + ex, 2)
+    parity_steps = sorted(
+        [(dy, m) for dy in range(side) for m in range(side // 2)],
+        key=lambda s: (-min(s[0], side - s[0]), -s[1]),
+    )
+
+    def of_parity(step):
+        return lax.rem(ey + step[0], side) * side + lax.rem(ex + shift + 2 * step[1], side)
+
+    same = lax.rem(e, 2) == core
+    unlike = lax.rem(e, 2) != core
+
     def in_column(step):
         return lax.rem(tz + step[0], deep) * 2 + lax.rem(core + step[1], 2)
 
@@ -136,13 +148,17 @@
         cp.start()
         return cp
 
-    mine256 = pl.multiple_of(core * 256, 128)
+    mine256 = pl.multiple_of(core * 256, 256)
     lx = load(x_h, xv, 0)
     small = [load(a, b, 11 + i) for i, (a, b) in enumerate([(again_h, again), (qg_h, qg), (kg_h, kg), (ho_h, ho), (lens_h, lens), (eg_h, eg), (routes_h, routes), (rw_h, rw)])]
-    lq = load(wq_h, wqkv.at[:, pl.ds(0, 256)], 1)
-    lk = load(wk_h, wqkv.at[:, pl.ds(256, 128)], 2)
-    lv = load(wv_h, wqkv.at[:, pl.ds(384, 128)], 3)
-    lo = load(wo_h, wo, 4)
+    at_q = wqkv.at[:, pl.ds(mine256, 256)]
+    at_k = wqkv.at[:, pl.ds(pl.multiple_of(mine256 + 512, 128), 128)]
+    at_v = wqkv.at[:, pl.ds(pl.multiple_of(mine256 + 640, 128), 128)]
+    at_o = wo.at[pl.ds(pl.multiple_of(core * 256, 256), 256), :]
+    lq = load(wq_h, at_q, 1)
+    lk = load(wk_h, at_k, 2)
+    lv = load(wv_h, at_v, 3)
+    lo = load(wo_h, at_o, 4)
     lkc = load(kc_h, kc, 5)
     lvc = load(vc_h, vc, 6)
     lg = load(gw_h.at[0], wgu.at[:, pl.ds(mine256, 128)], 7)
@@ -211,27 +227,71 @@
     xts[:, pl.ds(256, 128)] = jnp.where(lanes == 0, r0, jnp.where(lanes == 1, r1, 0.0))
 
     pl.semaphore_wait(bar, 2 * (n - 1))
-    for step in plane_steps(n):
-        p = in_plane(step)
-        remote(xn.at[:, cols_of(p)], xg.at[rows_of(e), :], 0, (p, t)).start()
-    xg[rows_of(e), :] = xn[:, cols_of(e)]
+
+    @pl.when(same)
+    def _():
+        for step in plane_steps(n):
+            p = in_plane(step)
+            remote(xn.at[:, cols_of(p)], xg.at[rows_of(e // 2), :], 0, (p, t)).start()
+        xg[rows_of(e // 2), :] = xn[:, cols_of(e)]
+
+    other = (e, tz * 2 + 1 - core)
+    swaps = [
+        remote(wq_h, at_q, 0, other, bsend, brecv),
+        remote(wk_h, at_k, 1, other, bsend, brecv),
+        remote(wv_h, at_v, 2, other, bsend, brecv),
+        remote(wo_h, at_o, 3, other, bsend, brecv),
+    ]
+    for cp in swaps:
+        cp.start()
+    others = pl.ds(0, n - 1)
+
+    def await_blocks(ref, sem, count):
+        @pl.when(same)
+        def _():
+            await_all(ref.at[pl.ds(0, count - 1)], sem)
+
+        @pl.when(unlike)
+        def _():
+            await_all(ref, sem)
+
     lq.wait()
+    swaps[0].wait_recv()
+
+    @pl.when(same)
+    def _():
+        await_all(xg.at[pl.ds(0, (deep - 1) * ROWS), :], rsem.at[0])
+
+    @pl.when(unlike)
+    def _():
+        await_all(xg, rsem.at[0])
+
+    def to_owners(part, dst, k):
+        for step in parity_steps:
+            b = of_parity(step)
+            for dc in (1, 0):
+                there = lax.rem(core + dc, 2)
+                cp = remote(part.at[rows_of(b // 2), cols_of(there)], dst.at[e], k, (b, tz * 2 + there))
+                if step != (0, 0) or dc == 1:
+                    cp.start()
+                    continue
+
+                @pl.when(unlike)
+                def _():
+                    cp.start()
+
+                @pl.when(same)
+                def _():
+                    dst[e] = part[rows_of(e // 2), cols_of(core)]
+
+    partq[...] = dot(xg[...], wqkv[:, pl.ds(0, 512)]).astype(BF16)
+    to_owners(partq, prq, 1)
     lk.wait()
     lv.wait()
-    others = pl.ds(0, n - 1)
-    other_rows = pl.ds(0, (n - 1) * ROWS)
-    await_all(xg.at[other_rows, :], rsem.at[0])
-
-    partq[...] = dot(xg[...], wqkv[:, pl.ds(0, 256)]).astype(BF16)
-    for step in plane_steps(n):
-        p = in_plane(step)
-        remote(partq.at[rows_of(p), :], prq.at[e], 1, (p, t)).start()
-    prq[e] = partq[rows_of(e), :]
-    partk[...] = dot(xg[...], wqkv[:, pl.ds(256, 256)]).astype(BF16)
-    for step in plane_steps(n):
-        p = in_plane(step)
-        remote(partk.at[rows_of(p), :], prk.at[e], 2, (p, t)).start()
-    prk[e] = partk[rows_of(e), :]
+    swaps[1].wait_recv()
+    swaps[2].wait_recv()
+    partk[...] = dot(xg[...], wqkv[:, pl.ds(512, 512)]).astype(BF16)
+    to_owners(partk, prk, 2)
 
     @pl.when(e != t)
     def _():
@@ -248,26 +308,25 @@
 
     def added(ref):
         total = ref[0].astype(F32)
-        for k in range(1, n):
+        for k in range(1, ref.shape[0]):
             total = total + ref[k].astype(F32)
         return total
 
-    await_all(prq.at[others], rsem.at[1])
-
-    other = (e, tz * 2 + 1 - core)
-    swaps = [
-        remote(gw_h.at[0], wgu.at[:, pl.ds(mine256, 128)], 0, other, bsend, brecv),
+    await_blocks(prq, rsem.at[1], n)
+
+    experts = [
+        remote(gw_h.at[0], wgu.at[:, pl.ds(mine256, 128)], 4, other, bsend, brecv),
         remote(
             uw_h.at[0],
             wgu.at[:, pl.ds(pl.multiple_of(mine256 + 128, 128), 128)],
-            1,
+            5,
             other,
             bsend,
             brecv,
         ),
-        remote(dw_h.at[0], dwp.at[core], 2, other, bsend, brecv),
+        remote(dw_h.at[0], dwp.at[core], 6, other, bsend, brecv),
     ]
-    for cp in swaps:
+    for cp in experts:
         cp.start()
 
     summed = added(prq)
@@ -316,11 +375,20 @@
     att[:, pl.ds(0, 128)] = attended[:ROWS].astype(BF16)
     att[:, pl.ds(128, 128)] = attended[ROWS:].astype(BF16)
 
+    heads = agb.at[rows_of(e // 2), cols_of(core)]
+    keeper = tz * 2 + lax.rem(e, 2)
     for step in plane_steps(n):
-        remote(att, agb.at[rows_of(e), :], 4, (in_plane(step), t)).start()
-    agb[rows_of(e), :] = att[...]
-
-    await_all(prk.at[others], rsem.at[2])
+        remote(att, heads, 4, (in_plane(step), keeper)).start()
+
+    @pl.when(unlike)
+    def _():
+        remote(att, heads, 4, other).start()
+
+    @pl.when(same)
+    def _():
+        agb[rows_of(e // 2), cols_of(core)] = att[...]
+
+    await_blocks(prk, rsem.at[2], n)
     summed = added(prk)
     fk[...] = head_norm(summed[:, 0:128], kg[...]).astype(BF16)
     fv[...] = summed[:, 128:256].astype(BF16)
@@ -333,14 +401,15 @@
     pt[...] = jnp.transpose(theirs, (1, 0)).astype(BF16)
 
     lo.wait()
-    await_all(agb.at[other_rows, :], rsem.at[4])
+    swaps[3].wait_recv()
+    await_blocks(prq, rsem.at[4], n)
 
     terms[...] = dot(agb[...], wo[...]).astype(BF16)
-    for step in column_steps(n):
-        p = in_column(step)
-        remote(terms.at[rows_of(p), :], rsb.at[t], 5, (e, p)).start()
-    rsb[t] = terms[rows_of(t), :]
-    await_all(rsb.at[others], rsem.at[5])
+    for dz in sorted(range(1, deep), key=lambda d: -min(d, deep - d)):
+        there = lax.rem(tz + dz, deep)
+        remote(terms.at[rows_of(there), :], rsb.at[tz], 5, (e, there * 2 + core)).start()
+    rsb[tz] = terms[rows_of(tz), :]
+    await_all(rsb.at[pl.ds(0, deep - 1)], rsem.at[5])
     residual = (xtr[:, pl.ds(0, 256)] + added(rsb)).astype(BF16)
     res_s[...] = residual
 
@@ -376,8 +445,8 @@
 
     lg.wait()
     lu.wait()
-    swaps[0].wait_recv()
-    swaps[1].wait_recv()
+    experts[0].wait_recv()
+    experts[1].wait_recv()
 
     all_but_one = pl.ds(0, deep * n - 1)
     await_all(xd.at[all_but_one], rsem.at[6])
@@ -413,7 +482,7 @@
     hidden0 = jnp.where(wide_first, hidden, 0.0).astype(BF16)
     hidden1 = jnp.where(wide_first, 0.0, hidden).astype(BF16)
     ld.wait()
-    swaps[2].wait_recv()
+    experts[2].wait_recv()
     down = dwp[...].reshape(256, width)
     for c in range(n):
         y = dot(hidden0, down[:, c * 256 : c * 256 + 128]) + dot(
@@ -452,16 +521,7 @@
     def _():
         remote(res_s, res_r, 7, (t, e)).wait_recv()
 
-    def await_returned(sem):
-        @pl.when(lax.rem(e, 2) != core)
-        def _():
-            await_all(rt, sem)
-
-        @pl.when(lax.rem(e, 2) == core)
-        def _():
-            await_all(rt.at[all_but_one], sem)
-
-    await_returned(rsem.at[8])
+    await_blocks(rt, rsem.at[8], deep * n)
     back = rt[pl.ds(0, n)].astype(F32)
     for k in range(1, deep):
         back = back + rt[pl.ds(k * n, n)].astype(F32)
@@ -470,14 +530,17 @@
     mixed = jnp.concatenate([mixed[:ROWS], mixed[ROWS:]], axis=1)
     out[...] = (res_r[...].astype(F32) + mixed).astype(BF16)
 
-    await_all(xg.at[other_rows, :], ssem.at[0])
-    await_all(prq.at[others], ssem.at[1])
-    await_all(prk.at[others], ssem.at[2])
-    await_all(agb.at[other_rows, :], ssem.at[4])
-    await_all(rsb.at[others], ssem.at[5])
+    @pl.when(same)
+    def _():
+        await_all(xn.at[:, pl.ds(0, (n - 1) * 256)], ssem.at[0])
+
+    await_blocks(prq, ssem.at[1], n)
+    await_blocks(prk, ssem.at[2], n)
+    await_blocks(prq, ssem.at[4], n)
+    await_all(rsb.at[pl.ds(0, deep - 1)], ssem.at[5])
     await_all(xd.at[all_but_one], ssem.at[6])
-    await_returned(ssem.at[8])
-    for cp in swaps:
+    await_blocks(rt, ssem.at[8], deep * n)
+    for cp in swaps + experts:
         cp.wait_send()
 
     @pl.when(e != t)
@@ -516,7 +579,7 @@
     width = hidden_in.shape[1]
     cache = key_cache.shape[1]
     vmem = pl.BlockSpec(memory_space=pltpu.VMEM)
-    hbm = pl.BlockSpec(memory_space=pl.ANY)
+    hbm = pl.BlockSpec(memory_space=pltpu.HBM)
     V = pltpu.VMEM
     I32 = jnp.int32
     deep = n // 2
@@ -531,19 +594,19 @@
         V((2, ROWS), F32),
         V((ROWS, width), BF16),
         V((ROWS, width), BF16),
-        V((n * ROWS, 256), BF16),
-        V((256, 512), BF16),
-        V((n * ROWS, 256), BF16),
-        V((n * ROWS, 256), BF16),
+        V((deep * ROWS, 256), BF16),
+        V((256, 1024), BF16),
+        V((deep * ROWS, 512), BF16),
+        V((deep * ROWS, 512), BF16),
         V((n, ROWS, 256), BF16),
         V((n, ROWS, 256), BF16),
         V((ROWS, cache, 128), BF16),
         V((ROWS, cache, 128), BF16),
         V((ROWS, 256), BF16),
-        V((n * ROWS, 256), BF16),
-        V((256, 256), BF16),
-        V((n * ROWS, 256), BF16),
-        V((n, ROWS, 256), BF16),
+        V((deep * ROWS, 512), BF16),
+        V((512, 256), BF16),
+        V((deep * ROWS, 256), BF16),
+        V((deep, ROWS, 256), BF16),
         V((ROWS, 384), F32),
         V((ROWS, 384), F32),
         V((ROWS, 256), BF16),
@@ -561,8 +624,8 @@
         pltpu.SemaphoreType.DMA((20,)),
         pltpu.SemaphoreType.DMA((9,)),
         pltpu.SemaphoreType.DMA((9,)),
-        pltpu.SemaphoreType.DMA((3,)),
-        pltpu.SemaphoreType.DMA((3,)),
+        pltpu.SemaphoreType.DMA((7,)),
+        pltpu.SemaphoreType.DMA((7,)),
     ]
     results = (
         jax.ShapeDtypeStruct((ROWS, 256), BF16),
@@ -571,7 +634,7 @@
     )
     made = pl.pallas_call(
         functools.partial(kernel, n),
-        out_shape=results,
+        out_shape=tuple(V(r.shape, r.dtype) for r in results),
         in_specs=[hbm] * 18,
         out_specs=(vmem, vmem, vmem),
         scratch_shapes=scratch,
@@ -600,7 +663,7 @@
     )
     return pl.pallas_call(
         emit, out_shape=results, in_specs=[vmem] * 3, out_specs=(vmem, vmem, vmem)
-    )(*made)
+    )(*[pltpu.with_memory_space_constraint(m, pltpu.VMEM) for m in made])
 
 
 def solution(mesh):

time: 59.7 us -> 56.5 us (0.946)
  Pallas kernels: 58.9 us -> 55.8 us
    pallas_call x1, Pallas kernels: 57.6 us -> 55.2 us  [body(): pl.pallas_call(functools.partial(kernel, n), out_shape=tuple((V(r.shape,...]
    pallas_call x1, Pallas kernels: 1.31 us -> 0.61 us  [body(): pl.pallas_call(emit, out_shape=results, in_specs=[vmem] * 3, out_specs=(v...]
where the time goes in v3:
time: 56.5 us
  Pallas kernels  55.8 us (99%)
  between operations  0.65 us (1%)
    pallas_call x1, Pallas kernels, body(): pl.pallas_call(functools.partial(kernel, n), out_shape=tuple((V(r.shape,...  55.2 us

profile of v3, /device:TPU:1, one launch (start us, length us, event | category | flops | bytes accessed | tf_op | source)
XLA Modules:
  0.0 56.5 jit_solution(15477283650518792694)
XLA Ops:
  0.6 55.2 %shard_map.193 = (bf16[16,256]{1,0:T(8,128)(2,1)S(1)}, bf16[16,128]{1,0:T(8,128)(2,1)S(1)}, bf16[16,128]{1,0:T(8,128)(2,1)S(1)}) custom-call(bf16[16,4096]{1,0:T(8,128)(2,1)} %x_h.1, f32[1,4096]{1,0:T(1,128)} %bitcast.8, bf16[256,256]{1,0:T(8,128)(2,1)} %wq_h.1, bf16[256,128]{1,0:T(8,128)(2,1)} %wk_h.1, bf16[256,128]{1,0:T(8,128)(2,1)} %wv_h.1, ...), custom_call_target="tpu_custom_call" | custom-call | tf_op jit(solution)/shard_map/pallas_call | solution.py:635
  55.9 0.6 %shard_map.194 = (bf16[16,256]{1,0:T(8,128)(2,1)}, bf16[16,128]{1,0:T(8,128)(2,1)}, bf16[16,128]{1,0:T(8,128)(2,1)}) custom-call(bf16[16,256]{1,0:T(8,128)(2,1)S(1)} %get-tuple-element.6.a, bf16[16,128]{1,0:T(8,128)(2,1)S(1)} %get-tuple-element.7.b, bf16[16,128]{1,0:T(8,128)(2,1)S(1)} %get-tuple-element.8.c), custom_call_target="tpu_custom_call" | custom-call | tf_op jit(solution)/shard_map/pallas_call | solution.py:664

commit v4 on v3

--- a/solution.py
+++ b/solution.py
@@ -228,6 +228,8 @@
 
     pl.semaphore_wait(bar, 2 * (n - 1))
 
+    keeper = tz * 2 + lax.rem(e, 2)
+
     @pl.when(same)
     def _():
         for step in plane_steps(n):
@@ -376,7 +378,6 @@
     att[:, pl.ds(128, 128)] = attended[ROWS:].astype(BF16)
 
     heads = agb.at[rows_of(e // 2), cols_of(core)]
-    keeper = tz * 2 + lax.rem(e, 2)
     for step in plane_steps(n):
         remote(att, heads, 4, (in_plane(step), keeper)).start()
 
@@ -419,20 +420,13 @@
         jnp.where(half == 0, picked[:, 0:128], picked[:, 128:256]).reshape(n, 8, 128).astype(BF16)
     )
 
-    def dispatch(dz):
-        there = lax.rem(tz + dz, deep) * 2 + core
-        for step in plane_steps(n):
-            p = in_plane(step)
-            remote(disp.at[p], xd.at[tz * n + e], 6, (p, there)).start()
-        return there
-
-    def dispatch_far(i, c):
-        there = dispatch(deep // 2 + (i + 1) // 2 * (2 * lax.rem(i, 2) - 1))
-        remote(disp.at[e], xd.at[tz * n + e], 6, (e, there)).start()
-        return c
-
-    lax.fori_loop(0, deep - 1, dispatch_far, 0)
-    dispatch(0)
+    far = sorted(range(1, deep), key=lambda d: -min(d, deep - d))
+    for step in plane_steps(n) + [(0, 0)]:
+        p = in_plane(step)
+        for dz in far + [0]:
+            if dz or step != (0, 0):
+                there = lax.rem(tz + dz, deep) * 2 + core
+                remote(disp.at[p], xd.at[tz * n + e], 6, (p, there)).start()
     xd[tz * n + e] = disp[e]
 
     @pl.when(e != t)
@@ -451,43 +445,38 @@
     all_but_one = pl.ds(0, deep * n - 1)
     await_all(xd.at[all_but_one], rsem.at[6])
 
-    squares = jnp.zeros((deep, 8, 128), F32)
     arrived = xd[...].reshape(deep, n, 8, 128)
+    first = (iota((deep * 8, 128), 0) // 4) % 2 == 0
+    squares = jnp.zeros((deep * 8, 128), F32)
+    total = jnp.zeros((deep * 8, 512), F32)
     for c in range(n):
         v = arrived[:, c].astype(F32)
-        squares = squares + v * v
-    squares = jnp.sum(squares, axis=2, keepdims=True)
-    squares = jnp.broadcast_to(squares, (deep, 8, 128)).reshape(deep * 8, 128)
+        square = v * v
+        squares = squares + square.reshape(deep * 8, 128)
+        v = (v * geb[c][None]).reshape(deep * 8, 128)
+        lhs = jnp.concatenate([jnp.where(first, v, 0.0), jnp.where(first, 0.0, v)], axis=1)
+        total = total + dot(lhs.astype(BF16), wgu[pl.ds(c * 256, 256), :])
 
     def both_halves(v):
         return jnp.concatenate(
             [v[i * 8 : i * 8 + 8] + pltpu.roll(v[i * 8 : i * 8 + 8], 4, 0) for i in range(deep)], axis=0
         )
 
+    squares = jnp.broadcast_to(jnp.sum(squares, axis=1, keepdims=True), (deep * 8, 128))
     scale = lax.rsqrt(both_halves(squares) * (1.0 / width) + EPSILON)
-    first = (iota((deep * 8, 128), 0) // 4) % 2 == 0
-    total = jnp.zeros((deep * 8, 512), F32)
-    for c in range(n):
-        v = (arrived[:, c].astype(F32) * geb[c][None]).reshape(deep * 8, 128)
-        v = v * scale
-        lhs = jnp.concatenate([jnp.where(first, v, 0.0), jnp.where(first, 0.0, v)], axis=1)
-        total = total + dot(lhs.astype(BF16), wgu[pl.ds(c * 256, 256), :])
     total = both_halves(total)
     hidden = []
     for k in range(2):
-        gate = total[:, k * 256 : k * 256 + 128]
-        hidden.append(gate * jax.nn.sigmoid(gate) * total[:, k * 256 + 128 : k * 256 + 256])
-    hidden = jnp.concatenate(hidden, axis=1)
-    wide_first = (iota((deep * 8, 256), 0) // 4) % 2 == 0
-    hidden0 = jnp.where(wide_first, hidden, 0.0).astype(BF16)
-    hidden1 = jnp.where(wide_first, 0.0, hidden).astype(BF16)
+        gate = total[:, k * 256 : k * 256 + 128] * scale
+        upward = total[:, k * 256 + 128 : k * 256 + 256] * scale
+        hidden.append(gate * jax.nn.sigmoid(gate) * upward)
+    hidden = jnp.concatenate(hidden, axis=1).astype(BF16)
     ld.wait()
     experts[2].wait_recv()
     down = dwp[...].reshape(256, width)
     for c in range(n):
-        y = dot(hidden0, down[:, c * 256 : c * 256 + 128]) + dot(
-            hidden1, down[:, c * 256 + 128 : c * 256 + 256]
-        )
+        y = dot(hidden, down[:, c * 256 : c * 256 + 256])
+        y = jnp.where(first, y[:, 0:128], y[:, 128:256])
         ys[:, c] = y.reshape(deep, 8, 128).astype(BF16)
 
     def give_back(dz, dc, skip):

time: 56.5 us -> 56.4 us (level)
  no operation moved by 1% of the time
where the time goes in v4:
time: 56.4 us; the launch traced here: 56.3 us
  Pallas kernels  55.6 us (99%)
  between operations  0.65 us (1%)
    pallas_call x1, Pallas kernels, body(): pl.pallas_call(functools.partial(kernel, n), out_shape=tuple((V(r.shape,...  55 us

profile of v4, /device:TPU:1, one launch (start us, length us, event | category | flops | bytes accessed | tf_op | source)
XLA Modules:
  0.0 56.3 jit_solution(2396281546332189260)
XLA Ops:
  0.6 55.0 %shard_map.193 = (bf16[16,256]{1,0:T(8,128)(2,1)S(1)}, bf16[16,128]{1,0:T(8,128)(2,1)S(1)}, bf16[16,128]{1,0:T(8,128)(2,1)S(1)}) custom-call(bf16[16,4096]{1,0:T(8,128)(2,1)} %x_h.1, f32[1,4096]{1,0:T(1,128)} %bitcast.8, bf16[256,256]{1,0:T(8,128)(2,1)} %wq_h.1, bf16[256,128]{1,0:T(8,128)(2,1)} %wk_h.1, bf16[256,128]{1,0:T(8,128)(2,1)} %wv_h.1, ...), custom_call_target="tpu_custom_call" | custom-call | tf_op jit(solution)/shard_map/pallas_call | solution.py:624
  55.7 0.6 %shard_map.194 = (bf16[16,256]{1,0:T(8,128)(2,1)}, bf16[16,128]{1,0:T(8,128)(2,1)}, bf16[16,128]{1,0:T(8,128)(2,1)}) custom-call(bf16[16,256]{1,0:T(8,128)(2,1)S(1)} %get-tuple-element.6.a, bf16[16,128]{1,0:T(8,128)(2,1)S(1)} %get-tuple-element.7.b, bf16[16,128]{1,0:T(8,128)(2,1)S(1)} %get-tuple-element.8.c), custom_call_target="tpu_custom_call" | custom-call | tf_op jit(solution)/shard_map/pallas_call | solution.py:653

commit v5 on v4

--- a/solution.py
+++ b/solution.py
@@ -185,12 +185,35 @@
         pltpu.make_async_copy(ref, ref, sem).wait()
 
     lx.wait()
-    for cp in small:
-        cp.wait()
+    small[0].wait()
     x = xv[...].astype(F32)
     meansq = jnp.sum(x * x, axis=1, keepdims=True) * (1.0 / width)
     xn[...] = (x * lax.rsqrt(meansq + EPSILON) * again[...]).astype(BF16)
 
+    pl.semaphore_wait(bar, 2 * (n - 1))
+
+    keeper = tz * 2 + lax.rem(e, 2)
+
+    @pl.when(same)
+    def _():
+        for step in plane_steps(n):
+            p = in_plane(step)
+            remote(xn.at[:, cols_of(p)], xg.at[rows_of(e // 2), :], 0, (p, t)).start()
+        xg[rows_of(e // 2), :] = xn[:, cols_of(e)]
+
+    other = (e, tz * 2 + 1 - core)
+    swaps = [
+        remote(wq_h, at_q, 0, other, bsend, brecv),
+        remote(wk_h, at_k, 1, other, bsend, brecv),
+        remote(wv_h, at_v, 2, other, bsend, brecv),
+        remote(wo_h, at_o, 3, other, bsend, brecv),
+    ]
+    for cp in swaps:
+        cp.start()
+    others = pl.ds(0, n - 1)
+
+    for cp in small[1:]:
+        cp.wait()
     tri[...] = (iota((256, 256), 0) >= iota((256, 256), 1)).astype(F32).astype(BF16)
     lane = iota((ROWS, 8 * n), 1)
     lower = (iota((ROWS, ROWS), 0) > iota((ROWS, ROWS), 1)).astype(F32).astype(BF16)
@@ -226,28 +249,6 @@
     lanes = iota((ROWS, 128), 1)
     xts[:, pl.ds(256, 128)] = jnp.where(lanes == 0, r0, jnp.where(lanes == 1, r1, 0.0))
 
-    pl.semaphore_wait(bar, 2 * (n - 1))
-
-    keeper = tz * 2 + lax.rem(e, 2)
-
-    @pl.when(same)
-    def _():
-        for step in plane_steps(n):
-            p = in_plane(step)
-            remote(xn.at[:, cols_of(p)], xg.at[rows_of(e // 2), :], 0, (p, t)).start()
-        xg[rows_of(e // 2), :] = xn[:, cols_of(e)]
-
-    other = (e, tz * 2 + 1 - core)
-    swaps = [
-        remote(wq_h, at_q, 0, other, bsend, brecv),
-        remote(wk_h, at_k, 1, other, bsend, brecv),
-        remote(wv_h, at_v, 2, other, bsend, brecv),
-        remote(wo_h, at_o, 3, other, bsend, brecv),
-    ]
-    for cp in swaps:
-        cp.start()
-    others = pl.ds(0, n - 1)
-
     def await_blocks(ref, sem, count):
         @pl.when(same)
         def _():
@@ -293,7 +294,6 @@
     swaps[1].wait_recv()
     swaps[2].wait_recv()
     partk[...] = dot(xg[...], wqkv[:, pl.ds(512, 512)]).astype(BF16)
-    to_owners(partk, prk, 2)
 
     @pl.when(e != t)
     def _():
@@ -389,11 +389,6 @@
     def _():
         agb[rows_of(e // 2), cols_of(core)] = att[...]
 
-    await_blocks(prk, rsem.at[2], n)
-    summed = added(prk)
-    fk[...] = head_norm(summed[:, 0:128], kg[...]).astype(BF16)
-    fv[...] = summed[:, 128:256].astype(BF16)
-
     @pl.when(e != t)
     def _():
         remote(xts, xtr, 3, (t, e)).wait_recv()
@@ -410,6 +405,8 @@
         there = lax.rem(tz + dz, deep)
         remote(terms.at[rows_of(there), :], rsb.at[tz], 5, (e, there * 2 + core)).start()
     rsb[tz] = terms[rows_of(tz), :]
+
+    to_owners(partk, prk, 2)
     await_all(rsb.at[pl.ds(0, deep - 1)], rsem.at[5])
     residual = (xtr[:, pl.ds(0, 256)] + added(rsb)).astype(BF16)
     res_s[...] = residual
@@ -505,6 +502,11 @@
     lax.fori_loop(0, deep - 1, give_far, 0)
     give_back(0, 1, False)
     give_back(0, 0, True)
+
+    await_blocks(prk, rsem.at[2], n)
+    summed = added(prk)
+    fk[...] = head_norm(summed[:, 0:128], kg[...]).astype(BF16)
+    fv[...] = summed[:, 128:256].astype(BF16)
 
     @pl.when(e != t)
     def _():

time: 56.4 us -> 55.9 us (level)
  no operation moved by 1% of the time
where the time goes in v5:
time: 55.9 us; the launch traced here: 55.8 us
  Pallas kernels  55.1 us (99%)
  between operations  0.65 us (1%)
    pallas_call x1, Pallas kernels, body(): pl.pallas_call(functools.partial(kernel, n), out_shape=tuple((V(r.shape,...  54.5 us

profile of v5, /device:TPU:1, one launch (start us, length us, event | category | flops | bytes accessed | tf_op | source)
XLA Modules:
  0.0 55.8 jit_solution(16404203918077324010)
XLA Ops:
  0.6 54.5 %shard_map.193 = (bf16[16,256]{1,0:T(8,128)(2,1)S(1)}, bf16[16,128]{1,0:T(8,128)(2,1)S(1)}, bf16[16,128]{1,0:T(8,128)(2,1)S(1)}) custom-call(bf16[16,4096]{1,0:T(8,128)(2,1)} %x_h.1, f32[1,4096]{1,0:T(1,128)} %bitcast.8, bf16[256,256]{1,0:T(8,128)(2,1)} %wq_h.1, bf16[256,128]{1,0:T(8,128)(2,1)} %wk_h.1, bf16[256,128]{1,0:T(8,128)(2,1)} %wv_h.1, ...), custom_call_target="tpu_custom_call" | custom-call | tf_op jit(solution)/shard_map/pallas_call | solution.py:626
  55.2 0.6 %shard_map.194 = (bf16[16,256]{1,0:T(8,128)(2,1)}, bf16[16,128]{1,0:T(8,128)(2,1)}, bf16[16,128]{1,0:T(8,128)(2,1)}) custom-call(bf16[16,256]{1,0:T(8,128)(2,1)S(1)} %get-tuple-element.6.a, bf16[16,128]{1,0:T(8,128)(2,1)S(1)} %get-tuple-element.7.b, bf16[16,128]{1,0:T(8,128)(2,1)S(1)} %get-tuple-element.8.c), custom_call_target="tpu_custom_call" | custom-call | tf_op jit(solution)/shard_map/pallas_call | solution.py:655

commit v6 on v5

--- a/solution.py
+++ b/solution.py
@@ -476,32 +476,23 @@
         y = jnp.where(first, y[:, 0:128], y[:, 128:256])
         ys[:, c] = y.reshape(deep, 8, 128).astype(BF16)
 
-    def give_back(dz, dc, skip):
-        there = lax.rem(tz + dz, deep) * 2 + lax.rem(core + dc, 2)
-        for i in range(deep):
-            b = 2 * i + core
-            cp = remote(ys.at[i, there], rt.at[tz * n + e], 8, (b, there))
-            if not skip:
-                cp.start()
-                continue
-
-            @pl.when(b != e)
-            def _():
-                cp.start()
-
-            @pl.when(b == e)
-            def _():
-                rt[tz * n + e] = ys[i, there]
-
-    def give_far(i, c):
-        dz = deep // 2 + (i + 1) // 2 * (2 * lax.rem(i, 2) - 1)
-        give_back(dz, 0, False)
-        give_back(dz, 1, False)
-        return c
-
-    lax.fori_loop(0, deep - 1, give_far, 0)
-    give_back(0, 1, False)
-    give_back(0, 0, True)
+    for step in parity_steps:
+        b = of_parity(step)
+        for dz in far + [0]:
+            for dc in (0, 1) if dz else (1, 0):
+                there = lax.rem(tz + dz, deep) * 2 + lax.rem(core + dc, 2)
+                cp = remote(ys.at[b // 2, there], rt.at[tz * n + e], 8, (b, there))
+                if step != (0, 0) or dz or dc:
+                    cp.start()
+                    continue
+
+                @pl.when(unlike)
+                def _():
+                    cp.start()
+
+                @pl.when(same)
+                def _():
+                    rt[tz * n + e] = ys[e // 2, t]
 
     await_blocks(prk, rsem.at[2], n)
     summed = added(prk)

time: 55.9 us -> 55.4 us (level)
  no operation moved by 1% of the time
where the time goes in v6:
time: 55.4 us; the launch traced here: 55.3 us
  Pallas kernels  54.7 us (99%)
  between operations  0.65 us (1%)
    pallas_call x1, Pallas kernels, body(): pl.pallas_call(functools.partial(kernel, n), out_shape=tuple((V(r.shape,...  54.1 us

profile of v6, /device:TPU:1, one launch (start us, length us, event | category | flops | bytes accessed | tf_op | source)
XLA Modules:
  0.0 55.3 jit_solution(7913855867583815076)
XLA Ops:
  0.6 54.1 %shard_map.193 = (bf16[16,256]{1,0:T(8,128)(2,1)S(1)}, bf16[16,128]{1,0:T(8,128)(2,1)S(1)}, bf16[16,128]{1,0:T(8,128)(2,1)S(1)}) custom-call(bf16[16,4096]{1,0:T(8,128)(2,1)} %x_h.1, f32[1,4096]{1,0:T(1,128)} %bitcast.8, bf16[256,256]{1,0:T(8,128)(2,1)} %wq_h.1, bf16[256,128]{1,0:T(8,128)(2,1)} %wk_h.1, bf16[256,128]{1,0:T(8,128)(2,1)} %wv_h.1, ...), custom_call_target="tpu_custom_call" | custom-call | tf_op jit(solution)/shard_map/pallas_call | solution.py:617
  54.7 0.6 %shard_map.194 = (bf16[16,256]{1,0:T(8,128)(2,1)}, bf16[16,128]{1,0:T(8,128)(2,1)}, bf16[16,128]{1,0:T(8,128)(2,1)}) custom-call(bf16[16,256]{1,0:T(8,128)(2,1)S(1)} %get-tuple-element.6.a, bf16[16,128]{1,0:T(8,128)(2,1)S(1)} %get-tuple-element.7.b, bf16[16,128]{1,0:T(8,128)(2,1)S(1)} %get-tuple-element.8.c), custom_call_target="tpu_custom_call" | custom-call | tf_op jit(solution)/shard_map/pallas_call | solution.py:646
